TPU v7x, 512 devices: a whole 4x8x8 slice. The times are simulated.
512 devices in a mesh: rep: 2 (over z_hi), fs: 32 (over z_lo, y), tp: 8 (over x, core).
Axes of the slice: x: 4, y: 8, z: 8 (z_hi: 2, z_lo: 4; z = z_hi * 4 + z_lo), core: 2. Of those that a mesh axis runs over, the one named last changes fastest.
Arguments:
- resid: bfloat16 [16384, 2048], P(('rep', 'fs'), 'tp'), may hold values from -6 to 6
- norm_gains: float32 [3, 2048], replicated, may hold values from 0.1 to 1.9
- gate_one: bfloat16 [2048, 5632], P('fs', 'tp'), may hold values from -0.125 to 0.125
- up_one: bfloat16 [2048, 5632], P('fs', 'tp'), may hold values from -0.125 to 0.125
- down_one: bfloat16 [5632, 2048], P('tp', 'fs'), may hold values from -0.15625 to 0.15625
- proj_u: bfloat16 [2048, 1024], P('fs', 'tp'), may hold values from -0.125 to 0.125
- proj_v: bfloat16 [2048, 1024], P('fs', 'tp'), may hold values from -0.125 to 0.125
- spatial: bfloat16 [8, 128, 128], P('tp'), may hold values from -0.5 to 0.5
- spatial_bias: float32 [8, 128], P('tp'), may hold values from 0.1 to 1.9
- mix_gain: float32 [1024], P('tp'), may hold values from 0.1 to 1.9
- head_gain: float32 [1024], P('tp'), may hold values from 0.1 to 1.9
- proj_out: bfloat16 [1024, 2048], P('tp', 'fs'), may hold values from -0.375 to 0.375
- gate_two: bfloat16 [2048, 5632], P('fs', 'tp'), may hold values from -0.125 to 0.125
- up_two: bfloat16 [2048, 5632], P('fs', 'tp'), may hold values from -0.125 to 0.125
- down_two: bfloat16 [5632, 2048], P('tp', 'fs'), may hold values from -0.15625 to 0.15625
Outputs:
- layer_out: bfloat16 [16384, 2048], P(('rep', 'fs'), 'tp')
All inputs are finite; a program needn't handle non-finite values.
Results may differ from a plain program's by a relative error of at most 0.019.
Values may be sent and summed in bfloat16 or wider, within the bound.
A program may use at most 64 MiB of HBM per device.

v0:
```python
import jax
import jax.numpy as jnp
from jax import lax
from jax.sharding import Mesh
from jax.sharding import PartitionSpec as P

HEAD_DIM = 128
BLOCK = 128
SPAN = 64
TP = ("tp_0", "tp_1")


def edges_of(length, count):
    turn = length // count
    if turn >= 8:
        turn -= turn % 8
    return [turn * k for k in range(1, count)]


def gather_in_order(value, axes, sequence):
    parts = value[None]
    for k in sequence:
        parts = lax.all_gather(parts, axes[k], axis=0, tiled=True)
    carried = [lax.axis_size(axes[k]) for k in reversed(sequence)]
    parts = parts.reshape(*carried, *value.shape)
    turned = sorted(range(len(sequence)), key=lambda place: sequence[len(sequence) - 1 - place])
    return parts.transpose(*turned, *range(len(sequence), parts.ndim)).reshape(-1, *value.shape)


def laid_out(parts, dim):
    shape = list(parts.shape[1:])
    shape[dim] *= parts.shape[0]
    return jnp.moveaxis(parts, 0, dim).reshape(shape)


def spread_gather(value, axes, dim):
    numbers = list(range(len(axes)))[::-1]
    widest = value.shape.index(max(value.shape[:-1] or value.shape))
    edges = [0, *edges_of(value.shape[widest], len(axes)), value.shape[widest]]
    finished = []
    for k, (start, end) in enumerate(zip(edges, edges[1:])):
        if end > start:
            slab = lax.slice_in_dim(value, start, end, axis=widest)
            finished.append(gather_in_order(slab, axes, numbers[k:] + numbers[:k]))
    return laid_out(jnp.concatenate(finished, axis=widest + 1), dim)


def sent_together(arrays, axis, dim, along):
    ends, at = ([], 0)
    for a in arrays[:-1]:
        at += a.shape[along]
        ends.append(at)
    both = jnp.concatenate(arrays, axis=along)
    return tuple(jnp.split(lax.all_gather(both, axis, axis=dim, tiled=True), ends, axis=along))


def split_up(value, dim, size):
    before, after = (value.shape[:dim], value.shape[dim + 1 :])
    return jnp.moveaxis(value.reshape(*before, size, -1, *after), dim, 0)


def summed_on_arrival(value, axis, dim):
    parts = split_up(value, dim, lax.axis_size(axis))
    arrived = lax.all_to_all(parts, axis, split_axis=0, concat_axis=0, tiled=True)
    return arrived.astype(jnp.float32).sum(axis=0)


def copy_for_each(value, axis):
    size = lax.axis_size(axis)
    return lax.all_to_all(
        jnp.broadcast_to(value[None], (size, *value.shape)), axis, 0, 0, tiled=True
    )


def gather_directly(value, axis, dim):
    parts = copy_for_each(value, axis)
    return laid_out(parts, dim)


def rms_scale(values, gain):
    return values * lax.rsqrt(jnp.mean(values * values, axis=-1, keepdims=True) + 1e-06) * gain


def normalized(stream, gain):
    whole = spread_gather(stream, TP, 1).astype(jnp.float32)
    return rms_scale(whole, gain).astype(jnp.bfloat16)


def accumulate(left, piece):
    return jnp.dot(left, piece, preferred_element_type=jnp.float32)


def folders(normed):

    def single(total, piece, start):
        return accumulate(normed, piece)

    def double(totals, pieces, start):
        return (accumulate(normed, pieces[0]), accumulate(normed, pieces[1]))

    return (single, double)


def ffn_inputs(normed, first_weight, second_weight):
    empty = jnp.zeros((normed.shape[0], first_weight.shape[1]), jnp.float32)
    single, double = folders(normed)
    result = double(
        (empty, empty), sent_together((first_weight, second_weight), "fs", 0, 1), jnp.int32(0)
    )
    return result


def mixer_inputs(normed, first_weight, second_weight):
    empty = jnp.zeros((normed.shape[0], first_weight.shape[1]), jnp.float32)
    single, double = folders(normed)
    result = double(
        (empty, empty), sent_together((first_weight, second_weight), "fs", 0, 1), jnp.int32(0)
    )
    return result


def feed_forward(stream, gain, gate_weight, up_weight, down_weight):
    normed = normalized(stream, gain)
    gate, up_part = ffn_inputs(normed, gate_weight, up_weight)
    hidden = (jax.nn.silu(gate) * up_part).astype(jnp.bfloat16)
    terms = jnp.dot(
        hidden,
        lax.all_gather(down_weight, "fs", axis=1, tiled=True),
        preferred_element_type=jnp.float32,
    )
    return summed_on_arrival(terms.astype(jnp.bfloat16), TP, 1)


def body(
    resid,
    norm_gains,
    gate_one,
    up_one,
    down_one,
    proj_u,
    proj_v,
    spatial,
    spatial_bias,
    mix_gain,
    head_gain,
    proj_out,
    gate_two,
    up_two,
    down_two,
):
    first = (
        resid.astype(jnp.float32)
        + 0.5 * feed_forward(resid, norm_gains[0], gate_one, up_one, down_one)
    ).astype(jnp.bfloat16)
    mnormed = normalized(first, norm_gains[1])
    u_part, v_part = mixer_inputs(mnormed, proj_u, proj_v)
    rows = u_part.shape[0]
    seqs = rows // BLOCK
    local_heads = spatial.shape[0]
    gated_u = jax.nn.gelu(u_part).reshape(seqs, BLOCK, local_heads, HEAD_DIM)
    gated_v = jax.nn.gelu(v_part).reshape(seqs, BLOCK, local_heads, HEAD_DIM)
    centre = jnp.mean(gated_v, axis=-1, keepdims=True)
    spread = jnp.mean(jnp.square(gated_v - centre), axis=-1, keepdims=True)
    vn = (
        (gated_v - centre) * lax.rsqrt(spread + 1e-05) * mix_gain.reshape(local_heads, HEAD_DIM)
    ).astype(jnp.bfloat16)
    segment = jnp.arange(BLOCK) // SPAN
    causal = segment[:, None] >= segment[None, :]
    masked = jnp.where(causal[None], spatial, jnp.zeros_like(spatial))
    mixed = (
        jnp.einsum("hts,bshd->bthd", masked, vn, preferred_element_type=jnp.float32)
        + spatial_bias.T[None, :, :, None]
    )
    product = gated_u * mixed
    gated = (
        rms_scale(product, head_gain.reshape(local_heads, HEAD_DIM))
        .astype(jnp.bfloat16)
        .reshape(rows, local_heads * HEAD_DIM)
    )
    terms = jnp.dot(gated, gather_directly(proj_out, "fs", 1), preferred_element_type=jnp.float32)
    branch = summed_on_arrival(terms.astype(jnp.bfloat16), TP, 1)
    second = (first.astype(jnp.float32) + branch).astype(jnp.bfloat16)
    return (
        second.astype(jnp.float32)
        + 0.5 * feed_forward(second, norm_gains[2], gate_two, up_two, down_two)
    ).astype(jnp.bfloat16)


def solution(mesh):
    finer = Mesh(
        mesh.devices.reshape(mesh.shape["rep"], mesh.shape["fs"], 4, 2),
        ("rep", "fs", "tp_0", "tp_1"),
    )
    in_specs = (
        P(("rep", "fs"), TP),
        P(),
        P("fs", TP),
        P("fs", TP),
        P(TP, "fs"),
        P("fs", TP),
        P("fs", TP),
        P(TP, None, None),
        P(TP, None),
        P(TP),
        P(TP),
        P(TP, "fs"),
        P("fs", TP),
        P("fs", TP),
        P(TP, "fs"),
    )
    out_specs = P(("rep", "fs"), TP)
    return jax.shard_map(body, mesh=finer, in_specs=in_specs, out_specs=out_specs, check_vma=False)
```

profile of v0, /device:TPU:1, one launch (start us, length us, event | category | flops | bytes accessed | tf_op | source)
XLA Modules:
  0.0 831.4 jit_solution(6896075159740473737)
XLA Ops:
  6.5 1.7 pad_maximum_fusion.3
  8.3 0.7 all-gather.14.cloned.1.call-update
  9.1 1.4 pad_maximum_fusion.5
  10.5 1.7 pad_maximum_fusion.4
  12.3 0.9 fusion.80
  13.2 10.5 %all-gather.1 = bf16[512,256]{1,0:T(8,128)(2,1)S(1)} all-gather(bf16[128,256]{1,0:T(8,128)(2,1)S(1)} %get-tuple-element.10), channel_id=3, replica_groups=mesh['rep'=2,'fs'=32,'tp_0'=4,'tp_1'=2] {'tp_0'}, dimensions={0}, use_global_device_ids=true | all-gather | bytes 327680 | tf_op jit(solution)/shard_map/all_gather | solution.py:23
  23.7 10.4 %all_gather.54 = bf16[8,128,256]{2,1,0:T(8,128)(2,1)S(1)} all-gather(bf16[4,128,256]{2,1,0:T(8,128)(2,1)S(1)} %bitcast.115), channel_id=1, replica_groups=mesh['rep'=2,'fs'=32,'tp_0'=4,'tp_1'=2] {'tp_1'}, dimensions={0}, use_global_device_ids=true | all-gather | bytes 786432 | tf_op jit(solution)/shard_map/all_gather | solution.py:23
  34.1 1.9 all-gather
  36.0 11.1 %all_gather.52 = bf16[8,128,256]{2,1,0:T(8,128)(2,1)S(1)} all-gather(bf16[2,128,256]{2,1,0:T(8,128)(2,1)S(1)} %bitcast.120), channel_id=1, replica_groups=mesh['rep'=2,'fs'=32,'tp_0'=4,'tp_1'=2] {'tp_0'}, dimensions={0}, use_global_device_ids=true | all-gather | bytes 655360 | tf_op jit(solution)/shard_map/all_gather | solution.py:23
  47.1 1.5 convert_bitcast_fusion.2
  48.6 1.9 copy.33
  50.6 0.3 fusion.8
  50.9 0.3 fusion.16
  51.2 105.9 %all-gather.12.cloned.1.call-done = bf16[2048,1408]{1,0:T(8,128)(2,1)} async-done(((bf16[64,1408]{1,0:T(8,128)(2,1)}), bf16[2048,1408]{1,0:T(8,128)(2,1)}) %all-gather.12.cloned.1.call-update) | async-done | bytes 5767184 | tf_op jit(solution)/shard_map/all_gather | solution.py:54
  157.1 3.2 fusion.6
  160.3 149.4 %all-gather.14.cloned.1.call-done = bf16[704,2048]{0,1:T(8,128)(2,1)} async-done(((bf16[704,64]{0,1:T(8,128)(2,1)}), bf16[704,2048]{0,1:T(8,128)(2,1)}) %all-gather.14.cloned.1.call-update) | async-done | bytes 2883600 | tf_op jit(solution)/shard_map/all_gather | solution.py:128
  309.7 7.2 convolution_convert_fusion.2
  316.9 1.1 copy.49
  318.0 26.7 %all-to-all-start = ((bf16[8,256,256]{2,1,0:T(8,128)(2,1)}), bf16[8,256,256]{2,1,0:T(8,128)(2,1)S(1)}, u32[]{:S(2)}, u32[]{:S(2)}) async-start(bf16[8,256,256]{2,1,0:T(8,128)(2,1)} %bitcast.101), calls=%async_computation | async-start | bytes 2097152 | tf_op jit(solution)/shard_map/all_to_all | solution.py:64
  344.7 0.6 all-gather.20.cloned.1.call-update
  345.3 14.5 %all-to-all-done = bf16[8,256,256]{2,1,0:T(8,128)(2,1)S(1)} async-done(((bf16[8,256,256]{2,1,0:T(8,128)(2,1)}), bf16[8,256,256]{2,1,0:T(8,128)(2,1)S(1)}, u32[]{:S(2)}, u32[]{:S(2)}) %all-to-all-start) | async-done | bytes 1048608 | tf_op jit(solution)/shard_map/all_to_all | solution.py:64
  359.8 0.9 broadcast_in_dim.41
  360.7 5.6 all-to-all-start.1
  366.6 10.5 %all-gather.3 = bf16[512,256]{1,0:T(8,128)(2,1)S(1)} all-gather(bf16[128,256]{1,0:T(8,128)(2,1)S(1)} %get-tuple-element.8), channel_id=5, replica_groups=mesh['rep'=2,'fs'=32,'tp_0'=4,'tp_1'=2] {'tp_0'}, dimensions={0}, use_global_device_ids=true | all-gather | bytes 327680 | tf_op jit(solution)/shard_map/all_gather | solution.py:23
  377.0 4.9 all_gather.60
  382.0 1.9 all-gather.2
  383.9 10.3 %all_gather.58 = bf16[8,128,256]{2,1,0:T(8,128)(2,1)S(1)} all-gather(bf16[2,128,256]{2,1,0:T(8,128)(2,1)S(1)} %bitcast.121), channel_id=1, replica_groups=mesh['rep'=2,'fs'=32,'tp_0'=4,'tp_1'=2] {'tp_0'}, dimensions={0}, use_global_device_ids=true | all-gather | bytes 655360 | tf_op jit(solution)/shard_map/all_gather | solution.py:23
  394.7 1.9 copy.36
  396.6 1.9 fusion.14
  398.5 63.0 %all-gather.16.cloned.1.call-done = bf16[2048,256]{1,0:T(8,128)(2,1)} async-done(((bf16[64,256]{1,0:T(8,128)(2,1)}), bf16[2048,256]{1,0:T(8,128)(2,1)}) %all-gather.16.cloned.1.call-update) | async-done | bytes 1048592 | tf_op jit(solution)/shard_map/all_gather | solution.py:54
  461.6 1.7 fusion.82
  463.6 0.5 fusion.58
  464.1 0.3 multiply_reduce_fusion
  464.6 0.4 convolution_convert_fusion
  465.1 42.0 %all_to_all.20 = bf16[8,256,256]{2,1,0:T(8,128)(2,1)S(1)} all-to-all(bf16[8,256,256]{2,1,0:T(8,128)(2,1)S(1)} %bitcast.109), channel_id=1, replica_groups=mesh['rep'=2,'fs'=32,'tp_0'=4,'tp_1'=2] {'tp_0','tp_1'}, dimensions={0} | all-to-all | bytes 2097152 | tf_op jit(solution)/shard_map/all_to_all | solution.py:64
  507.3 10.2 %all-gather.5 = bf16[512,256]{1,0:T(8,128)(2,1)S(1)} all-gather(bf16[128,256]{1,0:T(8,128)(2,1)S(1)} %get-tuple-element.6), channel_id=7, replica_groups=mesh['rep'=2,'fs'=32,'tp_0'=4,'tp_1'=2] {'tp_0'}, dimensions={0}, use_global_device_ids=true | all-gather | bytes 327680 | tf_op jit(solution)/shard_map/all_gather | solution.py:23
  517.5 5.0 all_gather.65
  522.4 1.9 all-gather.4
  524.4 10.6 %all_gather.63 = bf16[8,128,256]{2,1,0:T(8,128)(2,1)S(1)} all-gather(bf16[2,128,256]{2,1,0:T(8,128)(2,1)S(1)} %bitcast.122), channel_id=1, replica_groups=mesh['rep'=2,'fs'=32,'tp_0'=4,'tp_1'=2] {'tp_0'}, dimensions={0}, use_global_device_ids=true | all-gather | bytes 655360 | tf_op jit(solution)/shard_map/all_gather | solution.py:23
  535.0 1.6 convert_bitcast_fusion
  536.6 1.9 copy.39
  538.8 0.3 fusion.12
  539.1 83.7 %all-gather.18.cloned.1.call-done = bf16[2048,1408]{1,0:T(8,128)(2,1)} async-done(((bf16[64,1408]{1,0:T(8,128)(2,1)}), bf16[2048,1408]{1,0:T(8,128)(2,1)}) %all-gather.18.cloned.1.call-update) | async-done | bytes 5767184 | tf_op jit(solution)/shard_map/all_gather | solution.py:54
  622.8 3.2 fusion.2
  626.0 149.3 %all-gather.20.cloned.1.call-done = bf16[704,2048]{0,1:T(8,128)(2,1)} async-done(((bf16[704,64]{0,1:T(8,128)(2,1)}), bf16[704,2048]{0,1:T(8,128)(2,1)}) %all-gather.20.cloned.1.call-update) | async-done | bytes 2883600 | tf_op jit(solution)/shard_map/all_gather | solution.py:128
  775.4 7.2 convolution_convert_fusion.1
  782.7 41.3 %all_to_all.21 = bf16[8,256,256]{2,1,0:T(8,128)(2,1)S(1)} all-to-all(bf16[8,256,256]{2,1,0:T(8,128)(2,1)S(1)} %bitcast.110), channel_id=1, replica_groups=mesh['rep'=2,'fs'=32,'tp_0'=4,'tp_1'=2] {'tp_0','tp_1'}, dimensions={0} | all-to-all | bytes 2097152 | tf_op jit(solution)/shard_map/all_to_all | solution.py:64
  824.1 0.7 add_convert_fusion
  (51 shorter events, 2.2 us)
Async XLA Ops:
  6.5 150.6 %all-gather.12.cloned.1.call-start = ((), (), s32[]{:S(2)}) async-start(), calls=%async_computation.4 | async-start | bytes 5947392 | tf_op jit(solution)/shard_map/all_gather | solution.py:54
  8.3 301.4 %all-gather.14.cloned.1.call-start = ((), (), s32[]{:S(2)}) async-start(), calls=%async_computation.5 | async-start | bytes 3244032 | tf_op jit(solution)/shard_map/all_gather | solution.py:128
  9.0 452.5 %all-gather.16.cloned.1.call-start = ((), (), s32[]{:S(2)}) async-start(), calls=%async_computation.6 | async-start | bytes 1081344 | tf_op jit(solution)/shard_map/all_gather | solution.py:54
  10.5 612.4 %all-gather.18.cloned.1.call-start = ((), (), s32[]{:S(2)}) async-start(), calls=%async_computation.7 | async-start | bytes 5947392 | tf_op jit(solution)/shard_map/all_gather | solution.py:54
  48.6 2.2 copy-start.2
  316.9 42.9 %copy-start.3 = (bf16[128,64]{0,1:T(8,128)(2,1)S(1)}, bf16[128,64]{0,1:T(8,128)(2,1)}, u32[]{:S(2)}) copy-start(bf16[128,64]{0,1:T(8,128)(2,1)} %param.26) | copy-start | bytes 49156
  318.0 48.5 %copy-start = (bf16[256,256]{1,0:T(8,128)(2,1)S(1)}, bf16[256,256]{1,0:T(8,128)(2,1)}, u32[]{:S(2)}) copy-start(bf16[256,256]{1,0:T(8,128)(2,1)} %param.15) | copy-start | bytes 393220
  318.0 41.8 %all-to-all-start = ((bf16[8,256,256]{2,1,0:T(8,128)(2,1)}), bf16[8,256,256]{2,1,0:T(8,128)(2,1)S(1)}, u32[]{:S(2)}, u32[]{:S(2)}) async-start(bf16[8,256,256]{2,1,0:T(8,128)(2,1)} %bitcast.101), calls=%async_computation | async-start | bytes 2097152 | tf_op jit(solution)/shard_map/all_to_all | solution.py:64
  344.7 430.7 %all-gather.20.cloned.1.call-start = ((), (), s32[]{:S(2)}) async-start(), calls=%async_computation.8 | async-start | bytes 3244032 | tf_op jit(solution)/shard_map/all_gather | solution.py:128
  360.7 103.9 %all-to-all-start.1 = ((bf16[32,128,64]{1,2,0:T(8,128)(2,1)}), bf16[32,128,64]{1,2,0:T(8,128)(2,1)S(1)}, u32[]{:S(2)}, u32[]{:S(2)}) async-start(bf16[32,128,64]{1,2,0:T(8,128)(2,1)} %broadcast_in_dim.41), calls=%async_computation.1 | async-start | bytes 1048576 | tf_op jit(solution)/shard_map/all_to_all | solution.py:70
  396.6 66.9 %copy-start.4 = (f32[128]{0:T(128)S(1)}, f32[128]{0:T(128)}, u32[]{:S(2)}) copy-start(f32[128]{0:T(128)} %param.24) | copy-start | bytes 1540
  398.5 65.6 %copy-start.1 = (bf16[1,128,128]{2,1,0:T(8,128)(2,1)S(1)}, bf16[1,128,128]{2,1,0:T(8,128)(2,1)}, u32[]{:S(2)}) copy-start(bf16[1,128,128]{2,1,0:T(8,128)(2,1)} %param.22) | copy-start | bytes 98308
  398.5 65.6 %copy-start.5 = (f32[1,128]{1,0:T(1,128)S(1)}, f32[1,128]{1,0:T(1,128)}, u32[]{:S(2)}) copy-start(f32[1,128]{1,0:T(1,128)} %param.23) | copy-start | bytes 1540
  398.5 66.0 %copy-start.6 = (f32[128]{0:T(128)S(1)}, f32[128]{0:T(128)}, u32[]{:S(2)}) copy-start(f32[128]{0:T(128)} %param.25) | copy-start | bytes 1540
  461.6 2.1 copy-start.7
Sparse Core Ops, SparseCore 0:
  9.4 147.6 all-gather.11
  159.2 150.4 all-gather.13
  311.8 149.7 all-gather.15
  463.5 159.2 all-gather.17
  624.8 150.5 all-gather.19
where the time goes:
time: 832 us; the launch traced here: 831 us
  waiting for transfers between devices  567 us (68%)
  blocking collectives  172 us (21%)
  starting transfers between devices  32.5 us (4%)
  matrix products  23.8 us (3%)
  between operations  13.5 us (2%)
  other arithmetic  13.2 us (2%)
  local copies, waits for them, and re-layouts  8.94 us (1%)
    all_gather x2, waiting for transfers between devices, feed_forward(): lax.all_gather(down_weight, 'fs', axis=1, tiled=True)  299 us
    all_gather x3, waiting for transfers between devices, sent_together(): lax.all_gather(both, axis, axis=dim, tiled=True)  253 us
    all_gather x12, blocking collectives, gather_in_order(): parts = lax.all_gather(parts, axes[k], axis=0, tiled=True)  89.1 us
    all_to_all x2, blocking collectives, summed_on_arrival(): lax.all_to_all(parts, axis, split_axis=0, concat_axis=0, tiled=True)  83.3 us
    all_to_all x1, starting transfers between devices, summed_on_arrival(): lax.all_to_all(parts, axis, split_axis=0, concat_axis=0, tiled=True)  26.7 us
  transfers between devices with their start and end apart: 7, of which 6 were waited for; matrix products, arithmetic and copies ran while one was open for 4% of the time, Pallas kernels for 0%

commit v1 on v0

v1 whole, which is shorter than its diff:
```python
import functools
import heapq

import jax
import jax.numpy as jnp
from jax import lax
from jax.experimental import pallas as pl
from jax.experimental.pallas import tpu as pltpu
from jax.sharding import PartitionSpec as P

MESH = pl.DeviceIdType.MESH
BF16, F32 = jnp.bfloat16, jnp.float32
SHARD = 64
ITEMS = {
    "a1": (768, 32),
    "b1": (640, 48),
    "d1": (640, 48),
    "m": (512, 32),
    "a2": (768, 32),
    "b2": (640, 48),
    "d2": (640, 32),
}
NAMES = tuple(ITEMS)
RATE = {"y+": 46600.0, "y-": 46600.0, "z+": 46600.0, "z-": 46600.0, "x+": 46600.0, "x-": 46600.0, "d": 250000.0}
DELAY = {"d": 1.5}
AHEAD = 5.0
BLOCK_BYTES = 256 * 256 * 2
Y_FIRST, Z_FIRST = 0, 1
TWICE_UP = (-3, -1, 1, 3)


def rows_of(name, part):
    return ITEMS[name][1] if part == Y_FIRST else SHARD - ITEMS[name][1]


def children(part, dy, dz):
    out = []
    if part == Y_FIRST:
        if dz == 0:
            if 0 <= dy < 4:
                out.append(("y+", dy + 1, 0))
            if -3 < dy <= 0:
                out.append(("y-", dy - 1, 0))
            out += [("z+", dy, 1), ("z-", dy, -1)]
        elif dz == 1 and dy in TWICE_UP:
            out.append(("z+", dy, 2))
        elif dz == -1 and dy not in TWICE_UP:
            out.append(("z-", dy, -2))
    else:
        up, down = (4, 3) if dz == 2 else (3, 4)
        if dy == 0:
            if dz == 0:
                out += [("z+", 0, 1), ("z-", 0, -1)]
            elif dz == 1:
                out.append(("z+", 0, 2))
            out += [("y+", 1, dz), ("y-", -1, dz)]
        elif 0 < dy < up:
            out.append(("y+", dy + 1, dz))
        elif -down < dy < 0:
            out.append(("y-", dy - 1, dz))
    return out


def depth(part, dy, dz):
    return max((1 + depth(part, a, b) for _, a, b in children(part, dy, dz)), default=0)


def gather_steps(stage):
    block, half = BLOCK_BYTES, BLOCK_BYTES // 2
    return {
        "own": [("x+", block, "m1"), ("x-", block, "p1"), ("d", block, "end")],
        "m1": [("x+", half, "h0"), ("d", block, "end")],
        "p1": [("x-", half, "h1"), ("d", block, "end")],
        "h0": [("d", half, "end")],
        "h1": [("d", half, "end")],
    }


def chain():
    half = BLOCK_BYTES // 2
    steps = []
    for s in range(3):
        steps.append((("norm", s), [("ag", s)], 1.5, []))
        if s == 1:
            steps.append((("mix", s), [("w", "m")], 2.5, []))
        else:
            a, b, d = ("a1", "b1", "d1") if s == 0 else ("a2", "b2", "d2")
            for j in range(3):
                steps.append((("gu", s, j), [("w", a), ("w", b)], 1.0, []))
        needs = [("w", "m")] if s == 1 else [("w", d), ("w", "m")]
        for r in (2, 1, 3, 0):
            steps.append((("down", s, r, 1), needs, 0.4, [("d", BLOCK_BYTES, ("rs", s, "pr"), ("pr", s, r))]))
        for r in (2, 1, 3, 0):
            steps.append((("down", s, r, 0), [], 0.4, []))
        steps.append(
            (
                ("pair", s),
                [("rs", s, "pr")],
                0.8,
                [
                    ("x+", half, ("rs", s, "l0"), ("l0", s)),
                    ("x-", half, ("rs", s, "l1"), ("l1", s)),
                    ("x+", half, ("rs", s, "ra"), ("ra1", s)),
                    ("x-", half, ("rs", s, "rb"), ("rb0", s)),
                ],
            )
        )
        steps.append((("relay0", s), [("rs", s, "l0")], 0.2, [("x+", half, ("rs", s, "ra"), ("ra0", s))]))
        steps.append((("relay1", s), [("rs", s, "l1")], 0.2, [("x-", half, ("rs", s, "rb"), ("rb1", s))]))
        steps.append((("end", s), [("rs", s, "ra"), ("rs", s, "rb")], 0.4, [("next", s)]))
    return steps


@functools.lru_cache(None)
def plan():
    count = {}
    for name in NAMES:
        for part in (Y_FIRST, Z_FIRST):
            count[("w", name, part)] = 0

    def nodes(part, dy=0, dz=0):
        yield dy, dz
        for _, a, b in children(part, dy, dz):
            yield from nodes(part, a, b)

    for name in NAMES:
        for part in (Y_FIRST, Z_FIRST):
            count[("w", name, part)] = sum(not children(part, *n) for n in nodes(part))
    expected = {}
    for s in range(3):
        expected[("ag", s)] = 5
        expected[("rs", s, "pr")] = 4
        expected[("rs", s, "l0")] = expected[("rs", s, "l1")] = 1
        expected[("rs", s, "ra")] = expected[("rs", s, "rb")] = 2
    ops, now, serial = [], 0.0, 0
    free = {link: 0.0 for link in RATE}
    ready = {link: [] for link in RATE}
    arrivals, waited = [], set()

    def offer(link, priority, size, landing, op):
        nonlocal serial
        serial += 1
        heapq.heappush(ready[link], (priority, serial, size, landing, op))

    def offer_weight(index, name, part, dy, dz):
        for link, a, b in children(part, dy, dz):
            offer(
                link,
                (index, -depth(part, a, b)),
                rows_of(name, part) * ITEMS[name][0] * 2,
                ("w", index, name, part, a, b),
                ("send", name, part, dy, dz, link, a, b),
            )

    def offer_block(s, at):
        for link, size, landing in gather_steps(s)[at]:
            offer(link, (0, s), size, ("ag", s, landing), ("pass", s, at, link))

    def pump():
        nonlocal serial
        for link, queue in ready.items():
            while queue and free[link] - now < AHEAD:
                _, _, size, landing, op = heapq.heappop(queue)
                free[link] = max(free[link], now) + size / RATE[link]
                serial += 1
                heapq.heappush(arrivals, (free[link] + DELAY.get(link, 2.3), serial, landing))
                ops.append(op)

    for index, name in enumerate(NAMES):
        for part in (Y_FIRST, Z_FIRST):
            offer_weight(index, name, part, 0, 0)
    offer_block(0, "own")
    todo = chain()
    landed_all, times = 0, {}
    while todo or arrivals or any(ready.values()):
        while arrivals and arrivals[0][0] <= now:
            _, _, landing = heapq.heappop(arrivals)
            if landing[0] == "w":
                _, index, name, part, dy, dz = landing
                if children(part, dy, dz):
                    ops.append(("got", name, part, dy, dz))
                    offer_weight(index, name, part, dy, dz)
                else:
                    count[("w", name, part)] -= 1
            elif landing[0] == "ag" and landing[2] != "end":
                ops.append(("block", landing[1], landing[2]))
                offer_block(landing[1], landing[2])
            else:
                key = landing[:2] if landing[0] == "ag" else landing
                expected[key] -= 1
            times[landing[:3]] = now
        pump()
        if todo:
            step, needs, duration, sends = todo[0]
            done = True
            for need in needs:
                if need[0] == "w":
                    done &= count[("w", need[1], 0)] == 0 and count[("w", need[1], 1)] == 0
                else:
                    done &= expected[need] == 0
            if done:
                for need in needs:
                    if need not in waited:
                        waited.add(need)
                        ops.append(("all",) + need)
                ops.append(("do",) + step)
                times[step] = now
                now += duration
                todo.pop(0)
                for send in sends:
                    if send[0] == "next":
                        if send[1] < 2:
                            offer_block(send[1] + 1, "own")
                    else:
                        offer(send[0], (-1, 0), send[1], send[2], ("rsend",) + send[3])
                continue
        later = [arrivals[0][0]] if arrivals else []
        later += [free[link] - AHEAD + 0.01 for link, queue in ready.items() if queue]
        if not later:
            break
        now = max(min(later), now + 0.01)
    return ops, times, now


def semaphores():
    index, keys = {}, []
    for name in NAMES:
        for part in (Y_FIRST, Z_FIRST):
            index[("all", name, part)] = len(index)
            index[("sent", name, part)] = len(index)
    ops = plan()[0]
    for op in ops:
        if op[0] == "got":
            index[op[1:]] = len(index)
        elif op[0] == "block":
            index[op] = len(index)
        elif op[0] in ("pass", "rsend"):
            index[op] = len(index)
    for s in range(3):
        index[("ag", s)] = len(index)
        for what in ("pr", "l0", "l1", "ra", "rb"):
            index[("rs", s, what)] = len(index)
    return index


def rms_scale(values, mean_square, gain):
    return values * lax.rsqrt(mean_square + 1e-06) * gain


def contract(left, right):
    return lax.dot_general(left, right, (((1,), (1,)), ((), ())), preferred_element_type=F32)


def kernel(sems_of, *refs):
    weights_in = dict(zip(NAMES, refs[:7]))
    resid, gains, spatial, bias, mix_gain, head_gain, out = refs[7:14]
    g = dict(zip(NAMES, refs[14:21]))
    (xg, normed, hidden, ps, pr, po, sb, rl, ra, rb, tt, local_sem, sems) = refs[21:]

    rep, fs, tp = lax.axis_index("rep"), lax.axis_index("fs"), lax.axis_index("tp")
    x, core = tp // 2, tp % 2
    y, z = fs % 8, rep * 4 + fs // 8

    def device(link):
        if link[0] == "y":
            ny = (y + (1 if link[1] == "+" else 7)) % 8
            return {"rep": rep, "fs": (fs // 8) * 8 + ny, "tp": tp}
        if link[0] == "z":
            nz = (z + (1 if link[1] == "+" else 7)) % 8
            return {"rep": nz // 4, "fs": (nz % 4) * 8 + y, "tp": tp}
        if link[0] == "x":
            nx = (x + (1 if link[1] == "+" else 3)) % 4
            return {"rep": rep, "fs": fs, "tp": nx * 2 + core}
        return {"rep": rep, "fs": fs, "tp": x * 2 + 1 - core}

    devices = {link: device(link) for link in RATE}
    barrier = pltpu.get_barrier_semaphore()
    for link in RATE:
        pl.semaphore_signal(barrier, inc=1, device_id=devices[link], device_id_type=MESH)

    own = pl.multiple_of(fs * SHARD, SHARD)
    copies = [
        pltpu.make_async_copy(weights_in[name], g[name].at[pl.ds(own, SHARD)], local_sem.at[k])
        for k, name in enumerate(NAMES)
    ]
    copies.append(pltpu.make_async_copy(resid, xg.at[0, tp], local_sem.at[7]))
    for copy in copies:
        copy.start()
    pl.semaphore_wait(barrier, len(RATE))
    for copy in copies:
        copy.wait()

    def piece(name, part, dy, dz):
        f = ((z + 8 - dz) % 4) * 8 + (y + 8 - dy) % 8
        start = f * SHARD + (0 if part == Y_FIRST else ITEMS[name][1])
        return g[name].at[pl.ds(pl.multiple_of(start, 16), rows_of(name, part))]

    def remote(src, dst, send, recv, link):
        return pltpu.make_async_remote_copy(
            src_ref=src,
            dst_ref=dst,
            send_sem=sems.at[sems_of[send]],
            recv_sem=sems.at[sems_of[recv]],
            device_id=devices[link],
            device_id_type=MESH,
        )

    def wait_for(ref, key):
        pltpu.make_async_copy(ref, ref, sems.at[sems_of[key]]).wait()

    def block_at(s, at):
        shift = {"own": 0, "m1": 3, "p1": 1, "h0": 2, "h1": 2}[at]
        ref = xg.at[s, ((x + shift) % 4) * 2 + core]
        if at[0] == "h":
            return ref.at[pl.ds(0 if at == "h0" else 128, 128)]
        return ref

    def down(s, r, other):
        t = ((x + r) % 4) * 2 + (1 - core if other else core)
        at = pl.ds(pl.multiple_of(t * 256, 256), 256)
        if s == 1:
            total = contract(hidden[:, :128], g["m"][at, 256:384])
        else:
            total = contract(hidden[:, :640], g["d1" if s == 0 else "d2"][at, :])
            total = total + contract(hidden[:, 640:768], g["m"][at, 384:512])
        if other:
            ps[s, r] = total.astype(BF16)
        else:
            po[r] = total

    def gate_up(s, j):
        a, b = (g["a1"], g["b1"]) if s == 0 else (g["a2"], g["b2"])
        first = jnp.dot(normed[...], a[:, 256 * j : 256 * (j + 1)], preferred_element_type=F32)
        if j < 2:
            second = jnp.dot(normed[...], b[:, 256 * j : 256 * (j + 1)], preferred_element_type=F32)
            hidden[:, 256 * j : 256 * (j + 1)] = (jax.nn.silu(first) * second).astype(BF16)
            return
        second = jnp.dot(normed[...], b[:, 512:640], preferred_element_type=F32)
        hidden[:, 512:640] = (jax.nn.silu(first[:, :128]) * second).astype(BF16)
        rest = first[:, 128:]
        value = jax.nn.silu(rest) * pltpu.roll(rest, 64, 1)
        lane = lax.broadcasted_iota(jnp.int32, (256, 128), 1)
        keep = lane < 64 if s == 0 else lane >= 64
        hidden[:, 640:768] = jnp.where(keep, value, 0.0).astype(BF16)

    def norm(s):
        total = jnp.zeros((256, 1), F32)
        for t in range(8):
            values = xg[s, t].astype(F32)
            total = total + jnp.sum(values * values, axis=-1, keepdims=True)
        for t in range(8):
            cols = slice(256 * t, 256 * (t + 1))
            normed[:, cols] = rms_scale(xg[s, t].astype(F32), total / 2048.0, gains[s : s + 1, cols]).astype(BF16)

    def mix():
        both = jnp.dot(normed[...], g["m"][:, 0:256], preferred_element_type=F32)
        u, v = jax.nn.gelu(both[:, :128]), jax.nn.gelu(both[:, 128:])
        centre = jnp.mean(v, axis=-1, keepdims=True)
        spread = jnp.mean(jnp.square(v - centre), axis=-1, keepdims=True)
        vn = ((v - centre) * lax.rsqrt(spread + 1e-05) * mix_gain[...]).astype(BF16)
        to = lax.broadcasted_iota(jnp.int32, (128, 128), 0) // 64
        source = lax.broadcasted_iota(jnp.int32, (128, 128), 1) // 64
        masked = jnp.where(to >= source, spatial[...].astype(F32), 0.0).astype(BF16)
        for k in range(2):
            rows = slice(128 * k, 128 * (k + 1))
            mixed = jnp.dot(masked, vn[rows], preferred_element_type=F32) + bias[...]
            product = u[rows] * mixed
            square = jnp.mean(product * product, axis=-1, keepdims=True)
            hidden[rows, :128] = rms_scale(product, square, head_gain[...]).astype(BF16)

    lower, upper = pl.ds(0, 128), pl.ds(128, 128)
    for op in plan()[0]:
        kind = op[0]
        if kind == "send":
            _, name, part, dy, dz, link, a, b = op
            ref = piece(name, part, dy, dz)
            landing = (name, part, a, b) if children(part, a, b) else ("all", name, part)
            remote(ref, ref, ("sent", name, part), landing, link).start()
        elif kind == "got":
            _, name, part, dy, dz = op
            wait_for(piece(name, part, dy, dz), op[1:])
        elif kind == "pass":
            _, s, at, link = op
            ref = block_at(s, at)
            if link == "d":
                landing = ("ag", s)
            else:
                landing = ("block", s, {"own": {"x+": "m1", "x-": "p1"}, "m1": {"x+": "h0"}, "p1": {"x-": "h1"}}[at][link])
                if at == "m1":
                    ref = ref.at[lower]
                elif at == "p1":
                    ref = ref.at[upper]
            remote(ref, ref, op, landing, link).start()
        elif kind == "block":
            wait_for(block_at(op[1], op[2]), op)
        elif kind == "rsend":
            what, s = op[1], op[2]
            if what == "pr":
                remote(ps.at[s, op[3]], pr.at[s, op[3]], op, ("rs", s, "pr"), "d").start()
            elif what == "l0":
                remote(sb.at[s, 1, lower], rl.at[s, 0], op, ("rs", s, "l0"), "x+").start()
            elif what == "l1":
                remote(sb.at[s, 1, upper], rl.at[s, 1], op, ("rs", s, "l1"), "x-").start()
            elif what == "ra1":
                remote(sb.at[s, 0, upper], ra.at[s, upper], op, ("rs", s, "ra"), "x+").start()
            elif what == "rb0":
                remote(sb.at[s, 2, lower], rb.at[s, lower], op, ("rs", s, "rb"), "x-").start()
            elif what == "ra0":
                remote(tt.at[s, 0], ra.at[s, lower], op, ("rs", s, "ra"), "x+").start()
            elif what == "rb1":
                remote(tt.at[s, 1], rb.at[s, upper], op, ("rs", s, "rb"), "x-").start()
        elif kind == "all":
            if op[1] == "w":
                name = op[2]
                for part, many in ((Y_FIRST, 16), (Z_FIRST, 8)):
                    wait_for(g[name].at[pl.ds(0, many * rows_of(name, part))], ("all", name, part))
            elif op[1] == "ag":
                wait_for(xg.at[op[2], pl.ds(0, 4)], op[1:])
            else:
                _, _, s, what = op
                wait_for({"pr": pr.at[s], "l0": rl.at[s, 0], "l1": rl.at[s, 1], "ra": ra.at[s], "rb": rb.at[s]}[what], op[1:])
        else:
            what, s = op[1], op[2]
            if what == "norm":
                norm(s)
            elif what == "gu":
                gate_up(s, op[3])
            elif what == "mix":
                mix()
            elif what == "down":
                down(s, op[3], op[4])
            elif what == "pair":
                po[0] = po[0] + pr[s, 0].astype(F32)
                for r in (2, 1, 3):
                    sb[s, r - 1] = (po[r] + pr[s, r].astype(F32)).astype(BF16)
            elif what == "relay0":
                tt[s, 0] = (sb[s, 0, :128].astype(F32) + rl[s, 0].astype(F32)).astype(BF16)
            elif what == "relay1":
                tt[s, 1] = (sb[s, 2, 128:].astype(F32) + rl[s, 1].astype(F32)).astype(BF16)
            else:
                total = po[0] + ra[s].astype(F32) + rb[s].astype(F32)
                value = (xg[s, tp].astype(F32) + (1.0 if s == 1 else 0.5) * total).astype(BF16)
                if s < 2:
                    xg[s + 1, tp] = value
                else:
                    out[...] = value

    for name in NAMES:
        for part in (Y_FIRST, Z_FIRST):
            wait_for(g[name].at[pl.ds(0, 31 * rows_of(name, part))], ("sent", name, part))
    for op in plan()[0]:
        if op[0] == "pass":
            ref = block_at(op[1], op[2])
            if op[2] in ("m1", "p1") and op[3] != "d":
                ref = ref.at[lower]
            wait_for(ref, op)
        elif op[0] == "rsend":
            wait_for(ps.at[op[2], 0] if op[1] == "pr" else rl.at[op[2], 0], op)


def body(resid, norm_gains, gate_one, up_one, down_one, proj_u, proj_v, spatial, spatial_bias, mix_gain, head_gain, proj_out, gate_two, up_two, down_two):
    turned_one, turned_two = down_one.T, down_two.T
    weights = {
        "a1": jnp.concatenate([gate_one, up_one[:, 640:]], axis=1),
        "b1": up_one[:, :640],
        "d1": turned_one[:, :640],
        "m": jnp.concatenate([proj_u, proj_v, proj_out.T, turned_one[:, 640:], turned_two[:, 640:]], axis=1),
        "a2": jnp.concatenate([gate_two[:, :640], up_two[:, 640:], gate_two[:, 640:]], axis=1),
        "b2": up_two[:, :640],
        "d2": turned_two[:, :640],
    }
    sems_of = semaphores()
    rows, width = resid.shape
    anywhere = pl.BlockSpec(memory_space=pltpu.HBM)
    vmem = pl.BlockSpec(memory_space=pltpu.VMEM)
    return pl.pallas_call(
        functools.partial(kernel, sems_of),
        out_shape=jax.ShapeDtypeStruct((rows, width), BF16),
        in_specs=[anywhere] * 8 + [vmem] * 5,
        out_specs=vmem,
        scratch_shapes=[pltpu.VMEM((2048, ITEMS[name][0]), BF16) for name in NAMES]
        + [
            pltpu.VMEM((3, 8, 256, 256), BF16),
            pltpu.VMEM((256, 2048), BF16),
            pltpu.VMEM((256, 768), BF16),
            pltpu.VMEM((3, 4, 256, 256), BF16),
            pltpu.VMEM((3, 4, 256, 256), BF16),
            pltpu.VMEM((4, 256, 256), F32),
            pltpu.VMEM((3, 3, 256, 256), BF16),
            pltpu.VMEM((3, 2, 128, 256), BF16),
            pltpu.VMEM((3, 256, 256), BF16),
            pltpu.VMEM((3, 256, 256), BF16),
            pltpu.VMEM((3, 2, 128, 256), BF16),
            pltpu.SemaphoreType.DMA((8,)),
            pltpu.SemaphoreType.DMA((len(sems_of),)),
        ],
        compiler_params=pltpu.CompilerParams(collective_id=0, has_side_effects=True, vmem_limit_bytes=60 * 2**20),
        name="layer",
    )(
        *[weights[name] for name in NAMES],
        resid,
        norm_gains,
        spatial[0],
        spatial_bias.reshape(128, 1),
        mix_gain.reshape(1, 128),
        head_gain.reshape(1, 128),
    )


def solution(mesh):
    in_specs = (
        P(("rep", "fs"), "tp"),
        P(),
        P("fs", "tp"),
        P("fs", "tp"),
        P("tp", "fs"),
        P("fs", "tp"),
        P("fs", "tp"),
        P("tp", None, None),
        P("tp", None),
        P("tp"),
        P("tp"),
        P("tp", "fs"),
        P("fs", "tp"),
        P("fs", "tp"),
        P("tp", "fs"),
    )
    return jax.shard_map(body, mesh=mesh, in_specs=in_specs, out_specs=P(("rep", "fs"), "tp"), check_vma=False)
```

time: 832 us -> 171 us (0.21)
  waiting for transfers between devices: 567 us -> 0 us
  blocking collectives: 172 us -> 0 us
  Pallas kernels: 0 us -> 160 us
  starting transfers between devices: 32.5 us -> 0 us
  matrix products: 23.8 us -> 0 us
  between operations: 13.5 us -> 0.03 us
  other arithmetic: 13.2 us -> 0.76 us
    all_gather x5 -> x0, waiting for transfers between devices: 551 us -> none  [the longest x2 299 us: feed_forward(): lax.all_gather(down_weight, 'fs', axis=1, tiled=True)]
    pallas_call x0 -> x1, Pallas kernels: none -> 160 us  [body(): pl.pallas_call(functools.partial(kernel, sems_of), out_shape=jax.ShapeDty...]
    all_gather x12 -> x0, blocking collectives: 89.1 us -> none  [gather_in_order(): parts = lax.all_gather(parts, axes[k], axis=0, tiled=True)]
    all_to_all x2 -> x0, blocking collectives: 83.3 us -> none  [summed_on_arrival(): lax.all_to_all(parts, axis, split_axis=0, concat_axis=0, tiled=True)]
    all_to_all x2 -> x0, starting transfers between devices: 32.3 us -> none  [the longest x1 26.7 us: summed_on_arrival(): lax.all_to_all(parts, axis, split_axis=0, concat_axis=0, tiled=True)]
    dot_general x8 -> x0, matrix products: 23.8 us -> none  [the longest x2 14.4 us: feed_forward(): jnp.dot(hidden, lax.all_gather(down_weight, 'fs', axis=1, tiled=True), pr...]
    all_to_all x2 -> x0, waiting for transfers between devices: 14.5 us -> none  [the longest x1 14.5 us: summed_on_arrival(): lax.all_to_all(parts, axis, split_axis=0, concat_axis=0, tiled=True)]
  transfers between devices with their start and end apart: 7 -> 0, of which waited for: 6 -> 0; matrix products, arithmetic and copies ran while one was open for 4% -> 0% of each run, Pallas kernels for 0% -> 0%
where the time goes in v1:
time: 171 us; the launch traced here: 170 us
  Pallas kernels  160 us (94%)
  local copies, waits for them, and re-layouts  9.37 us (5%)
    pallas_call x1, Pallas kernels, body(): pl.pallas_call(functools.partial(kernel, sems_of), out_shape=jax.ShapeDty...  160 us

profile of v1, /device:TPU:1, one launch (start us, length us, event | category | flops | bytes accessed | tf_op | source)
XLA Modules:
  0.0 170.4 jit_solution(17106344035050029799)
XLA Ops:
  0.0 0.7 slice.41
  0.7 0.7 slice.42
  1.4 0.0 copy-start.7
  1.4 0.0 copy-start.5
  1.4 0.0 copy-start.6
  1.4 0.7 copy-done.7
  2.2 0.0 copy-done.5
  2.2 0.0 copy-done.6
  2.2 0.0 copy-start.8
  2.2 0.0 copy-start
  2.2 0.7 concatenate.10.refs_3_
  2.9 0.0 copy-done.8
  2.9 0.7 copy.16.refs_10_
  3.6 0.0 copy-done
  3.6 0.0 copy-start.1
  3.6 0.6 slice.40.refs_2_
  4.3 0.3 copy-done.1
  4.6 0.0 copy-start.2
  4.6 0.6 slice.43.refs_6_
  5.2 0.3 copy-done.2
  5.5 0.0 copy-start.4
  5.5 0.6 slice.31.refs_1_
  6.1 0.0 slice-start
  6.1 0.0 slice-start.1
  6.1 0.0 slice-start.2
  6.1 0.0 slice-start.3
  6.1 0.3 copy-done.4
  6.4 0.5 slice-done
  6.9 0.2 slice-done.1
  7.1 0.0 slice-done.2
  7.1 0.0 slice-done.3
  7.1 0.0 copy-start.3
  7.1 0.8 pad_maximum_fusion
  7.8 0.1 copy-done.3
  8.0 0.6 slice.38.refs_5_
  8.6 160.2 %layer.1 = bf16[256,256]{1,0:T(8,128)(2,1)} custom-call(bf16[64,768]{1,0:T(8,128)(2,1)} %get-tuple-element.5.refs_0_, bf16[64,640]{1,0:T(8,128)(2,1)} %slice.31.refs_1_, bf16[64,640]{1,0:T(8,128)(2,1)} %slice.40.refs_2_, bf16[64,512]{1,0:T(8,128)(2,1)} %concatenate.10.refs_3_, bf16[64,768]{1,0:T(8,128)(2,1)} %get-tuple-element.6.refs_4_, ...), custom_call_target="tpu_custom_call" | custom-call | tf_op jit(solution)/shard_map/layer/pallas_call | solution.py:476
  168.8 1.6 copy.18
Async XLA Ops:
  1.4 0.7 copy-start.7
  1.4 0.7 copy-start.5
  1.4 0.7 copy-start.6
  2.2 0.7 copy-start.8
  2.2 1.4 copy-start
  3.6 0.9 copy-start.1
  4.6 0.9 copy-start.2
  5.5 0.9 copy-start.4
  6.1 0.7 slice-start
  6.1 0.9 slice-start.1
  6.1 0.9 slice-start.2
  6.1 0.9 slice-start.3
  7.1 0.9 copy-start.3

commit v2 on v1

v2 whole, which is shorter than its diff:
```python
import functools
import heapq

import jax
import jax.numpy as jnp
from jax import lax
from jax.experimental import pallas as pl
from jax.experimental.pallas import tpu as pltpu
from jax.sharding import PartitionSpec as P

MESH = pl.DeviceIdType.MESH
BF16, F32 = jnp.bfloat16, jnp.float32
SHARD = 64
ITEMS = {
    "a1": (768, 32),
    "b1": (640, 48),
    "d1": (768, 32),
    "m": (384, 48),
    "a2": (768, 32),
    "b2": (640, 48),
    "d2": (640, 32),
}
NAMES = tuple(ITEMS)
RATE = {"y+": 46600.0, "y-": 46600.0, "z+": 46600.0, "z-": 46600.0, "x+": 46600.0, "x-": 46600.0, "d": 250000.0}
DELAY = {"d": 1.5}
AHEAD = 2.0
ROWS = 128
HALF = 64
BLOCK_BYTES = ROWS * 256 * 2
STREAMS = 2
Y_FIRST, Z_FIRST = 0, 1
TWICE_UP = (-3, -1, 1, 3)


def rows_of(name, part):
    return ITEMS[name][1] if part == Y_FIRST else SHARD - ITEMS[name][1]


def children(part, dy, dz):
    out = []
    if part == Y_FIRST:
        if dz == 0:
            if 0 <= dy < 4:
                out.append(("y+", dy + 1, 0))
            if -3 < dy <= 0:
                out.append(("y-", dy - 1, 0))
            out += [("z+", dy, 1), ("z-", dy, -1)]
        elif dz == 1 and dy in TWICE_UP:
            out.append(("z+", dy, 2))
        elif dz == -1 and dy not in TWICE_UP:
            out.append(("z-", dy, -2))
    else:
        up, down = (4, 3) if dz == 2 else (3, 4)
        if dy == 0:
            if dz == 0:
                out += [("z+", 0, 1), ("z-", 0, -1)]
            elif dz == 1:
                out.append(("z+", 0, 2))
            out += [("y+", 1, dz), ("y-", -1, dz)]
        elif 0 < dy < up:
            out.append(("y+", dy + 1, dz))
        elif -down < dy < 0:
            out.append(("y-", dy - 1, dz))
    return out


def depth(part, dy, dz):
    return max((1 + depth(part, a, b) for _, a, b in children(part, dy, dz)), default=0)


def gather_steps():
    block, half = BLOCK_BYTES, BLOCK_BYTES // 2
    return {
        "own": [("x+", block, "m1"), ("x-", block, "p1"), ("d", block, "end")],
        "m1": [("x+", half, "h0"), ("d", block, "end")],
        "p1": [("x-", half, "h1"), ("d", block, "end")],
        "h0": [("d", half, "end")],
        "h1": [("d", half, "end")],
    }


def chain(h):
    half = BLOCK_BYTES // 2
    steps = []
    for s in range(3):
        steps.append((("norm", s, h), [("ag", s, h)], 0.8, []))
        if s == 1:
            steps.append((("mix", s, h), [("w", "m")], 1.3, []))
        else:
            a, b, d = ("a1", "b1", "d1") if s == 0 else ("a2", "b2", "d2")
            for j in range(3):
                steps.append((("gu", s, h, j), [("w", a), ("w", b)], 0.6, []))
        needs = [("w", "m")] if s == 1 else [("w", "d1"), ("w", d)]
        for r in (2, 1, 3, 0):
            steps.append((("down", s, h, r, 1), needs, 0.25, [("d", BLOCK_BYTES, ("rs", s, h, "pr"), ("pr", s, h, r))]))
        for r in (2, 1, 3, 0):
            steps.append((("down", s, h, r, 0), [], 0.25, []))
        key = ("rs", s, h)
        steps.append(
            (
                ("pair", s, h),
                [key + ("pr",)],
                0.5,
                [
                    ("x+", half, key + ("l0",), ("l0", s, h)),
                    ("x-", half, key + ("l1",), ("l1", s, h)),
                    ("x+", half, key + ("ra",), ("ra1", s, h)),
                    ("x-", half, key + ("rb",), ("rb0", s, h)),
                ],
            )
        )
        steps.append((("relay0", s, h), [key + ("l0",)], 0.15, [("x+", half, key + ("ra",), ("ra0", s, h))]))
        steps.append((("relay1", s, h), [key + ("l1",)], 0.15, [("x-", half, key + ("rb",), ("rb1", s, h))]))
        steps.append((("end", s, h), [key + ("ra",), key + ("rb",)], 0.3, [("next", s)]))
    return steps


@functools.lru_cache(None)
def plan():
    count = {}
    for name in NAMES:
        for part in (Y_FIRST, Z_FIRST):
            count[("w", name, part)] = 0

    def nodes(part, dy=0, dz=0):
        yield dy, dz
        for _, a, b in children(part, dy, dz):
            yield from nodes(part, a, b)

    for name in NAMES:
        for part in (Y_FIRST, Z_FIRST):
            count[("w", name, part)] = sum(not children(part, *n) for n in nodes(part))
    expected = {}
    for s in range(3):
        for h in range(STREAMS):
            expected[("ag", s, h)] = 5
            expected[("rs", s, h, "pr")] = 4
            expected[("rs", s, h, "l0")] = expected[("rs", s, h, "l1")] = 1
            expected[("rs", s, h, "ra")] = expected[("rs", s, h, "rb")] = 2
    ops, now, serial = [], 0.0, 0
    free = {link: 0.0 for link in RATE}
    ready = {link: [] for link in RATE}
    arrivals, waited = [], set()

    def offer(link, priority, size, landing, op):
        nonlocal serial
        serial += 1
        heapq.heappush(ready[link], (priority, serial, size, landing, op))

    def offer_weight(index, name, part, dy, dz):
        for link, a, b in children(part, dy, dz):
            offer(
                link,
                (index, -depth(part, a, b)),
                rows_of(name, part) * ITEMS[name][0] * 2,
                ("w", index, name, part, a, b),
                ("send", name, part, dy, dz, link, a, b),
            )

    def offer_block(s, h, at):
        for link, size, landing in gather_steps()[at]:
            offer(link, (h, s), size, ("ag", s, h, landing), ("pass", s, h, at, link))

    def pump():
        nonlocal serial
        for link, queue in ready.items():
            while queue and free[link] - now < AHEAD:
                _, _, size, landing, op = heapq.heappop(queue)
                free[link] = max(free[link], now) + size / RATE[link]
                serial += 1
                heapq.heappush(arrivals, (free[link] + DELAY.get(link, 2.3), serial, landing))
                ops.append(op)

    for index, name in enumerate(NAMES):
        for part in (Y_FIRST, Z_FIRST):
            offer_weight(index, name, part, 0, 0)
    for h in range(STREAMS):
        offer_block(0, h, "own")
    chains = [chain(h) for h in range(STREAMS)]
    times = {}
    while any(chains) or arrivals or any(ready.values()):
        while arrivals and arrivals[0][0] <= now:
            _, _, landing = heapq.heappop(arrivals)
            if landing[0] == "w":
                _, index, name, part, dy, dz = landing
                if children(part, dy, dz):
                    ops.append(("got", name, part, dy, dz))
                    offer_weight(index, name, part, dy, dz)
                else:
                    count[("w", name, part)] -= 1
            elif landing[0] == "ag" and landing[3] != "end":
                ops.append(("block",) + landing[1:])
                offer_block(*landing[1:])
            else:
                key = landing[:3] if landing[0] == "ag" else landing
                expected[key] -= 1
            times[landing[:3]] = now
        pump()
        ran = False
        for h, todo in enumerate(chains):
            if not todo:
                continue
            step, needs, duration, sends = todo[0]
            done = True
            for need in needs:
                if need[0] == "w":
                    done &= count[("w", need[1], 0)] == 0 and count[("w", need[1], 1)] == 0
                else:
                    done &= expected[need] == 0
            if not done:
                continue
            for need in needs:
                if need not in waited:
                    waited.add(need)
                    ops.append(("all",) + need)
            ops.append(("do",) + step)
            times[step] = now
            now += duration
            todo.pop(0)
            for send in sends:
                if send[0] == "next":
                    if send[1] < 2:
                        offer_block(send[1] + 1, h, "own")
                else:
                    offer(send[0], (-1, 0), send[1], send[2], ("rsend",) + send[3])
            ran = True
            break
        if ran:
            continue
        later = [arrivals[0][0]] if arrivals else []
        later += [free[link] - AHEAD + 0.01 for link, queue in ready.items() if queue]
        if not later:
            break
        now = max(min(later), now + 0.01)
    return ops, times, now


def semaphores():
    index, keys = {}, []
    for name in NAMES:
        for part in (Y_FIRST, Z_FIRST):
            index[("all", name, part)] = len(index)
            index[("sent", name, part)] = len(index)
    ops = plan()[0]
    for op in ops:
        if op[0] == "got":
            index[op[1:]] = len(index)
        elif op[0] == "block":
            index[op] = len(index)
        elif op[0] in ("pass", "rsend"):
            index[op] = len(index)
    for s in range(3):
        for h in range(STREAMS):
            index[("ag", s, h)] = len(index)
            for what in ("pr", "l0", "l1", "ra", "rb"):
                index[("rs", s, h, what)] = len(index)
    return index


def rms_scale(values, mean_square, gain):
    return values * lax.rsqrt(mean_square + 1e-06) * gain


def contract(left, right):
    return lax.dot_general(left, right, (((1,), (1,)), ((), ())), preferred_element_type=F32)


def kernel(sems_of, *refs):
    gate_one, up_one, down_one, proj_u, proj_v, proj_out, gate_two, up_two, down_two = refs[:9]
    resid, small_in, out = refs[9], refs[10:15], refs[15]
    g = dict(zip(NAMES, refs[16:23]))
    (xg, normed, hidden, ps, pr, po, sb, rl, ra, rb, tt) = refs[23:34]
    raw, small, local_sem, sems = refs[34:41], refs[41:46], refs[46], refs[47]
    gains, spatial, bias, mix_gain, head_gain = small

    rep, fs, tp = lax.axis_index("rep"), lax.axis_index("fs"), lax.axis_index("tp")
    x, core = tp // 2, tp % 2
    y, z = fs % 8, rep * 4 + fs // 8

    def device(link):
        if link[0] == "y":
            ny = (y + (1 if link[1] == "+" else 7)) % 8
            return {"rep": rep, "fs": (fs // 8) * 8 + ny, "tp": tp}
        if link[0] == "z":
            nz = (z + (1 if link[1] == "+" else 7)) % 8
            return {"rep": nz // 4, "fs": (nz % 4) * 8 + y, "tp": tp}
        if link[0] == "x":
            nx = (x + (1 if link[1] == "+" else 3)) % 4
            return {"rep": rep, "fs": fs, "tp": nx * 2 + core}
        return {"rep": rep, "fs": fs, "tp": x * 2 + 1 - core}

    devices = {link: device(link) for link in RATE}
    barrier = pltpu.get_barrier_semaphore()
    for link in RATE:
        pl.semaphore_signal(barrier, inc=1, device_id=devices[link], device_id_type=MESH)

    own = pl.multiple_of(fs * SHARD, SHARD)
    rows = pl.ds(own, SHARD)
    pairs = [
        (up_one.at[:, pl.ds(0, 640)], g["b1"].at[rows]),
        (gate_one.at[:, pl.ds(0, 640)], g["a1"].at[rows, pl.ds(0, 640)]),
        (up_two.at[:, pl.ds(0, 640)], g["b2"].at[rows]),
        (gate_two.at[:, pl.ds(0, 640)], g["a2"].at[rows, pl.ds(0, 640)]),
        (proj_u, g["m"].at[rows, pl.ds(0, 128)]),
        (proj_v, g["m"].at[rows, pl.ds(128, 128)]),
        (resid, xg.at[0, tp]),
    ]
    first_copies = len(pairs)
    pairs += list(zip((gate_one, up_one, gate_two, up_two, down_one, down_two, proj_out), raw))
    pairs += list(zip(small_in, small))
    copies = [pltpu.make_async_copy(src, dst, local_sem.at[k]) for k, (src, dst) in enumerate(pairs)]
    for copy in copies[first_copies:] + copies[:first_copies]:
        copy.start()
    for copy in copies[first_copies:]:
        copy.wait()
    one = jnp.where(
        lax.broadcasted_iota(jnp.int32, (SHARD, SHARD), 0) == lax.broadcasted_iota(jnp.int32, (SHARD, SHARD), 1), 1.0, 0.0
    ).astype(BF16)

    def turned(ref):
        return contract(one, ref[...]).astype(BF16)

    g["a1"][rows, 640:768] = jnp.concatenate([raw[0][:, 640:704], raw[1][:, 640:704]], axis=1)
    g["a2"][rows, 640:768] = jnp.concatenate([raw[3][:, 640:704], raw[2][:, 640:704]], axis=1)
    down_a, down_b = turned(raw[4]), turned(raw[5])
    g["d1"][rows, 0:640] = down_a[:, :640]
    g["d1"][rows, 640:768] = jnp.concatenate([down_a[:, 640:704], down_b[:, 640:704]], axis=1)
    g["d2"][rows, :] = down_b[:, :640]
    g["m"][rows, 256:384] = turned(raw[6])
    pl.semaphore_wait(barrier, len(RATE))
    for copy in copies[:first_copies]:
        copy.wait()

    def piece(name, part, dy, dz):
        f = ((z + 8 - dz) % 4) * 8 + (y + 8 - dy) % 8
        start = f * SHARD + (0 if part == Y_FIRST else ITEMS[name][1])
        return g[name].at[pl.ds(pl.multiple_of(start, 16), rows_of(name, part))]

    def remote(src, dst, send, recv, link):
        return pltpu.make_async_remote_copy(
            src_ref=src,
            dst_ref=dst,
            send_sem=sems.at[sems_of[send]],
            recv_sem=sems.at[sems_of[recv]],
            device_id=devices[link],
            device_id_type=MESH,
        )

    def wait_for(ref, key):
        pltpu.make_async_copy(ref, ref, sems.at[sems_of[key]]).wait()

    def block_at(s, h, at):
        shift = {"own": 0, "m1": 3, "p1": 1, "h0": 2, "h1": 2}[at]
        start, size = h * ROWS, ROWS
        if at[0] == "h":
            start, size = start + (0 if at == "h0" else HALF), HALF
        return xg.at[s, ((x + shift) % 4) * 2 + core, pl.ds(start, size)]

    def down(s, h, r, other):
        t = ((x + r) % 4) * 2 + (1 - core if other else core)
        at = pl.ds(pl.multiple_of(t * 256, 256), 256)
        if s == 1:
            total = contract(hidden[h, :, :128], g["m"][at, 256:384])
        elif s == 0:
            total = contract(hidden[h], g["d1"][at, :])
        else:
            total = contract(hidden[h, :, :640], g["d2"][at, :])
            total = total + contract(hidden[h, :, 640:768], g["d1"][at, 640:768])
        if other:
            ps[s, h, r] = total.astype(BF16)
        else:
            po[h, r] = total

    def gate_up(s, h, j):
        a, b = (g["a1"], g["b1"]) if s == 0 else (g["a2"], g["b2"])
        first = jnp.dot(normed[h], a[:, 256 * j : 256 * (j + 1)], preferred_element_type=F32)
        if j < 2:
            second = jnp.dot(normed[h], b[:, 256 * j : 256 * (j + 1)], preferred_element_type=F32)
            hidden[h, :, 256 * j : 256 * (j + 1)] = (jax.nn.silu(first) * second).astype(BF16)
            return
        second = jnp.dot(normed[h], b[:, 512:640], preferred_element_type=F32)
        hidden[h, :, 512:640] = (jax.nn.silu(first[:, :128]) * second).astype(BF16)
        rest = first[:, 128:]
        value = jax.nn.silu(rest) * pltpu.roll(rest, 64, 1)
        lane = lax.broadcasted_iota(jnp.int32, (ROWS, 128), 1)
        keep = lane < 64 if s == 0 else lane >= 64
        hidden[h, :, 640:768] = jnp.where(keep, value, 0.0).astype(BF16)

    def norm(s, h):
        rows = slice(h * ROWS, (h + 1) * ROWS)
        total = jnp.zeros((ROWS, 1), F32)
        for t in range(8):
            values = xg[s, t, rows].astype(F32)
            total = total + jnp.sum(values * values, axis=-1, keepdims=True)
        for t in range(8):
            cols = slice(256 * t, 256 * (t + 1))
            scaled = rms_scale(xg[s, t, rows].astype(F32), total / 2048.0, gains[s : s + 1, cols])
            normed[h, :, cols] = scaled.astype(BF16)

    def mix(h):
        both = jnp.dot(normed[h], g["m"][:, 0:256], preferred_element_type=F32)
        u, v = jax.nn.gelu(both[:, :128]), jax.nn.gelu(both[:, 128:])
        centre = jnp.mean(v, axis=-1, keepdims=True)
        spread = jnp.mean(jnp.square(v - centre), axis=-1, keepdims=True)
        vn = ((v - centre) * lax.rsqrt(spread + 1e-05) * mix_gain[...]).astype(BF16)
        to, source = lax.broadcasted_iota(jnp.int32, (128, 128), 0), lax.broadcasted_iota(jnp.int32, (128, 128), 1)
        masked = jnp.where(to // 64 >= source // 64, spatial[0].astype(F32), 0.0).astype(BF16)
        offset = jnp.sum(jnp.where(to == source, bias[...], 0.0), axis=-1, keepdims=True)
        product = u * (jnp.dot(masked, vn, preferred_element_type=F32) + offset)
        square = jnp.mean(product * product, axis=-1, keepdims=True)
        hidden[h, :, :128] = rms_scale(product, square, head_gain[...]).astype(BF16)

    lower, upper = pl.ds(0, HALF), pl.ds(HALF, HALF)
    for op in plan()[0]:
        kind = op[0]
        if kind == "send":
            _, name, part, dy, dz, link, a, b = op
            ref = piece(name, part, dy, dz)
            landing = (name, part, a, b) if children(part, a, b) else ("all", name, part)
            remote(ref, ref, ("sent", name, part), landing, link).start()
        elif kind == "got":
            _, name, part, dy, dz = op
            wait_for(piece(name, part, dy, dz), op[1:])
        elif kind == "pass":
            _, s, h, at, link = op
            ref = block_at(s, h, at)
            if link == "d":
                landing = ("ag", s, h)
            else:
                arrived = {"own": {"x+": "m1", "x-": "p1"}, "m1": {"x+": "h0"}, "p1": {"x-": "h1"}}[at][link]
                landing = ("block", s, h, arrived)
                if at == "m1":
                    ref = ref.at[lower]
                elif at == "p1":
                    ref = ref.at[upper]
            remote(ref, ref, op, landing, link).start()
        elif kind == "block":
            wait_for(block_at(*op[1:]), op)
        elif kind == "rsend":
            what, s, h = op[1:4]
            key = ("rs", s, h)
            if what == "pr":
                remote(ps.at[s, h, op[4]], pr.at[s, h, op[4]], op, key + ("pr",), "d").start()
            elif what == "l0":
                remote(sb.at[s, h, 1, lower], rl.at[s, h, 0], op, key + ("l0",), "x+").start()
            elif what == "l1":
                remote(sb.at[s, h, 1, upper], rl.at[s, h, 1], op, key + ("l1",), "x-").start()
            elif what == "ra1":
                remote(sb.at[s, h, 0, upper], ra.at[s, h, upper], op, key + ("ra",), "x+").start()
            elif what == "rb0":
                remote(sb.at[s, h, 2, lower], rb.at[s, h, lower], op, key + ("rb",), "x-").start()
            elif what == "ra0":
                remote(tt.at[s, h, 0], ra.at[s, h, lower], op, key + ("ra",), "x+").start()
            elif what == "rb1":
                remote(tt.at[s, h, 1], rb.at[s, h, upper], op, key + ("rb",), "x-").start()
        elif kind == "all":
            if op[1] == "w":
                name = op[2]
                for part, many in ((Y_FIRST, 16), (Z_FIRST, 8)):
                    wait_for(g[name].at[pl.ds(0, many * rows_of(name, part))], ("all", name, part))
            elif op[1] == "ag":
                wait_for(xg.at[op[2], pl.ds(0, 4), pl.ds(op[3] * ROWS, ROWS)], op[1:])
            else:
                _, _, s, h, what = op
                at = {"pr": pr.at[s, h], "l0": rl.at[s, h, 0], "l1": rl.at[s, h, 1], "ra": ra.at[s, h], "rb": rb.at[s, h]}
                wait_for(at[what], op[1:])
        else:
            what, s, h = op[1:4]
            if what == "norm":
                norm(s, h)
            elif what == "gu":
                gate_up(s, h, op[4])
            elif what == "mix":
                mix(h)
            elif what == "down":
                down(s, h, op[4], op[5])
            elif what == "pair":
                po[h, 0] = po[h, 0] + pr[s, h, 0].astype(F32)
                for r in (2, 1, 3):
                    sb[s, h, r - 1] = (po[h, r] + pr[s, h, r].astype(F32)).astype(BF16)
            elif what == "relay0":
                tt[s, h, 0] = (sb[s, h, 0, :HALF].astype(F32) + rl[s, h, 0].astype(F32)).astype(BF16)
            elif what == "relay1":
                tt[s, h, 1] = (sb[s, h, 2, HALF:].astype(F32) + rl[s, h, 1].astype(F32)).astype(BF16)
            else:
                at = slice(h * ROWS, (h + 1) * ROWS)
                total = po[h, 0] + ra[s, h].astype(F32) + rb[s, h].astype(F32)
                value = (xg[s, tp, at].astype(F32) + (1.0 if s == 1 else 0.5) * total).astype(BF16)
                if s < 2:
                    xg[s + 1, tp, at] = value
                else:
                    out[at, :] = value

    for name in NAMES:
        for part in (Y_FIRST, Z_FIRST):
            wait_for(g[name].at[pl.ds(0, 31 * rows_of(name, part))], ("sent", name, part))
    for op in plan()[0]:
        if op[0] == "pass":
            ref = block_at(op[1], op[2], op[3])
            if op[3] in ("m1", "p1") and op[4] != "d":
                ref = ref.at[lower]
            wait_for(ref, op)
        elif op[0] == "rsend":
            wait_for(ps.at[op[2], op[3], 0] if op[1] == "pr" else rl.at[op[2], op[3], 0], op)


def body(resid, norm_gains, gate_one, up_one, down_one, proj_u, proj_v, spatial, spatial_bias, mix_gain, head_gain, proj_out, gate_two, up_two, down_two):
    weights = (gate_one, up_one, down_one, proj_u, proj_v, proj_out, gate_two, up_two, down_two)
    small = (norm_gains, spatial, spatial_bias, mix_gain.reshape(1, 128), head_gain.reshape(1, 128))
    raw = (gate_one, up_one, gate_two, up_two, down_one, down_two, proj_out)
    sems_of = semaphores()
    rows, width = resid.shape
    return pl.pallas_call(
        functools.partial(kernel, sems_of),
        out_shape=jax.ShapeDtypeStruct((rows, width), BF16),
        in_specs=[pl.BlockSpec(memory_space=pltpu.HBM)] * 15,
        out_specs=pl.BlockSpec(memory_space=pltpu.VMEM),
        scratch_shapes=[pltpu.VMEM((2048, ITEMS[name][0]), BF16) for name in NAMES]
        + [
            pltpu.VMEM((3, 8, 256, 256), BF16),
            pltpu.VMEM((STREAMS, ROWS, 2048), BF16),
            pltpu.VMEM((STREAMS, ROWS, 768), BF16),
            pltpu.VMEM((3, STREAMS, 4, ROWS, 256), BF16),
            pltpu.VMEM((3, STREAMS, 4, ROWS, 256), BF16),
            pltpu.VMEM((STREAMS, 4, ROWS, 256), F32),
            pltpu.VMEM((3, STREAMS, 3, ROWS, 256), BF16),
            pltpu.VMEM((3, STREAMS, 2, HALF, 256), BF16),
            pltpu.VMEM((3, STREAMS, ROWS, 256), BF16),
            pltpu.VMEM((3, STREAMS, ROWS, 256), BF16),
            pltpu.VMEM((3, STREAMS, 2, HALF, 256), BF16),
        ]
        + [pltpu.VMEM(a.shape, a.dtype) for a in raw + small]
        + [pltpu.SemaphoreType.DMA((19,)), pltpu.SemaphoreType.DMA((len(sems_of),))],
        compiler_params=pltpu.CompilerParams(collective_id=0, has_side_effects=True, vmem_limit_bytes=60 * 2**20),
        name="layer",
    )(*weights, resid, *small)


def solution(mesh):
    in_specs = (
        P(("rep", "fs"), "tp"),
        P(),
        P("fs", "tp"),
        P("fs", "tp"),
        P("tp", "fs"),
        P("fs", "tp"),
        P("fs", "tp"),
        P("tp", None, None),
        P("tp", None),
        P("tp"),
        P("tp"),
        P("tp", "fs"),
        P("fs", "tp"),
        P("fs", "tp"),
        P("tp", "fs"),
    )
    return jax.shard_map(body, mesh=mesh, in_specs=in_specs, out_specs=P(("rep", "fs"), "tp"), check_vma=False)
```

time: 171 us -> 140 us (0.82)
  Pallas kernels: 160 us -> 134 us
  local copies, waits for them, and re-layouts: 9.37 us -> 5.54 us
    pallas_call x1, Pallas kernels: 160 us -> 134 us  [body(): pl.pallas_call(functools.partial(kernel, sems_of), out_shape=jax.ShapeDty...]
    slice x14 -> x0, local copies, waits for them, and re-layouts: 4.63 us -> none  [the longest x1 0.72 us: body(): turned_one[:, 640:]]
    unnamed x19 -> x6, local copies, waits for them, and re-layouts: 3.3 us -> 5.54 us
where the time goes in v2:
time: 140 us
  Pallas kernels  134 us (96%)
  local copies, waits for them, and re-layouts  5.54 us (4%)
    pallas_call x1, Pallas kernels, body(): pl.pallas_call(functools.partial(kernel, sems_of), out_shape=jax.ShapeDty...  134 us
    unnamed x6, local copies, waits for them, and re-layouts  5.54 us

profile of v2, /device:TPU:1, one launch (start us, length us, event | category | flops | bytes accessed | tf_op | source)
XLA Modules:
  0.0 139.6 jit_solution(13249396093257466427)
XLA Ops:
  0.0 1.4 %copy.17.refs_5_ = bf16[128,64]{1,0:T(8,128)(2,1)} copy(bf16[128,64]{0,1:T(8,128)(2,1)} %param.26) | data formatting | bytes 32768 | tf_op args[11]
  1.4 0.0 copy-start
  1.4 1.7 %copy.16.refs_2_ = bf16[704,64]{1,0:T(8,128)(2,1)} copy(bf16[704,64]{0,1:T(8,128)(2,1)} %param.19) | data formatting | bytes 180224 | tf_op args[4]
  3.2 0.0 copy-done
  3.2 0.8 copy.18.refs_8_
  4.0 134.0 %layer.1 = bf16[256,256]{1,0:T(8,128)(2,1)} custom-call(bf16[64,704]{1,0:T(8,128)(2,1)} %refs_0_.1, bf16[64,704]{1,0:T(8,128)(2,1)} %refs_1_.1, bf16[704,64]{1,0:T(8,128)(2,1)} %copy.16.refs_2_, bf16[64,128]{1,0:T(8,128)(2,1)} %refs_3_.1, bf16[64,128]{1,0:T(8,128)(2,1)} %refs_4_.1, bf16[128,64]{1,0:T(8,128)(2,1)} %copy.17.refs_5_, bf16[64,704]{1,0:T(8,128)(2,1)} %refs_6_.1, ...), custom_call_target="tpu_custom_call" | custom-call | tf_op jit(solution)/shard_map/layer/pallas_call | solution.py:513
  138.0 1.6 %copy.20 = bf16[256,256]{1,0:T(8,128)(2,1)} copy(bf16[256,256]{1,0:T(8,128)(2,1)} %layer.1) | data formatting | bytes 262144
Async XLA Ops:
  1.4 1.7 %copy-start = (bf16[704,64]{0,1:T(8,128)(2,1)S(1)}, bf16[704,64]{0,1:T(8,128)(2,1)}, u32[]{:S(2)}) copy-start(bf16[704,64]{0,1:T(8,128)(2,1)} %param.29) | copy-start | bytes 270340

commit v3 on v2

v3 whole, which is shorter than its diff:
```python
import functools
import heapq

import jax
import jax.numpy as jnp
from jax import lax
from jax.experimental import pallas as pl
from jax.experimental.pallas import tpu as pltpu
from jax.sharding import PartitionSpec as P

MESH = pl.DeviceIdType.MESH
BF16, F32 = jnp.bfloat16, jnp.float32
SHARD = 64
ITEMS = {
    "a1": (768, 48),
    "d1": (384, 48),
    "m": (512, 48),
    "a2": (768, 32),
    "b2": (640, 48),
    "d2": (640, 32),
}
NAMES = tuple(ITEMS)
SPLIT = ("a1", "d1")
TURN = {"a1": 0, "d1": 0, "m": 1, "a2": 2, "b2": 2, "d2": 2}
RATE = {"y+": 46600.0, "y-": 46600.0, "z+": 46600.0, "z-": 46600.0, "x+": 46600.0, "x-": 46600.0, "d": 250000.0, "q": 30000.0}
DELAY = {"d": 1.5}
GREET = ("y+", "y-", "z+", "z-", "x+", "x-", "d")
AHEAD = 1.5
ROWS = 128
HALF = 64
BLOCK_BYTES = ROWS * 256 * 2
STREAMS = 4
Y_FIRST, Z_FIRST, Y_SAME, Y_CROSS, Z_SAME, Z_CROSS = range(6)
TWICE_UP = (-3, -1, 1, 3)


def parts_of(name):
    return (Y_SAME, Y_CROSS, Z_SAME, Z_CROSS) if name in SPLIT else (Y_FIRST, Z_FIRST)


def y_first(part):
    return part in (Y_FIRST, Y_SAME, Y_CROSS)


def rows_of(name, part):
    return ITEMS[name][1] if y_first(part) else SHARD - ITEMS[name][1]


def needed(part, dy):
    return part in (Y_FIRST, Z_FIRST) or (dy % 2 == 0) == (part in (Y_SAME, Z_SAME))


def reach(part, dz):
    if part in (Y_SAME, Z_SAME):
        return (4, 2) if dz in (0, 2) else (2, 4)
    if part in (Y_CROSS, Z_CROSS):
        return 3, 3
    return (4, 3) if y_first(part) or dz == 2 else (3, 4)


def children(part, dy, dz):
    out = []
    up, down = reach(part, dz)
    if y_first(part):
        if dz == 0:
            if 0 <= dy < up:
                out.append(("y+", dy + 1, 0))
            if -down < dy <= 0:
                out.append(("y-", dy - 1, 0))
            if needed(part, dy):
                out += [("z+", dy, 1), ("z-", dy, -1)]
        elif dz == 1 and dy in UP[part]:
            out.append(("z+", dy, 2))
        elif dz == -1 and dy not in UP[part]:
            out.append(("z-", dy, -2))
    elif dy == 0:
        if dz == 0:
            out += [("z+", 0, 1), ("z-", 0, -1)]
        elif dz == 1 and part != Z_CROSS:
            out.append(("z+", 0, 2))
        elif dz == -1 and part == Z_CROSS:
            out.append(("z-", 0, -2))
        out += [("y+", 1, dz), ("y-", -1, dz)]
    elif 0 < dy < up:
        out.append(("y+", dy + 1, dz))
    elif -down < dy < 0:
        out.append(("y-", dy - 1, dz))
    return out


UP = {Y_FIRST: (-3, -1, 1, 3), Y_SAME: (0, 4), Y_CROSS: (-1, 1)}


def last_ones(part):
    ends = total = 0
    todo = [(0, 0)]
    while todo:
        here = todo.pop()
        after = children(part, *here)
        ends += not after
        total += 1
        todo += [(a, b) for _, a, b in after]
    return ends, total - 1


def depth(part, dy, dz):
    return max((1 + depth(part, a, b) for _, a, b in children(part, dy, dz)), default=0)


def gather_steps():
    block, half = BLOCK_BYTES, BLOCK_BYTES // 2
    return {
        "own": [("x+", block, "m1"), ("x-", block, "p1"), ("d", block, "end")],
        "m1": [("x+", half, "h0"), ("d", block, "end")],
        "p1": [("x-", half, "h1"), ("d", block, "end")],
        "h0": [("d", half, "end")],
        "h1": [("d", half, "end")],
    }


def chain(h):
    half = BLOCK_BYTES // 2
    steps = []
    for s in range(3 if h < 2 else 1):
        steps.append((("norm", s, h), [("ag", s, h)], 0.35, []))
        if s == 1:
            steps.append((("mix", s, h), [("w", "m")], 0.7, []))
        elif s == 0:
            steps.append((("gu", s, h, 0), [("w", "a1")], 0.5, []))
        else:
            for j in range(3):
                steps.append((("gu", s, h, j), [("w", "a2"), ("w", "b2")], 0.3, []))
        needs = [[("w", "d1")], [("w", "m")], [("w", "m"), ("w", "d2")]][s]
        for r in (2, 1, 3, 0):
            steps.append((("down", s, h, r, 1), needs, 0.1, [("d", BLOCK_BYTES, ("rs", s, h, "pr"), ("pr", s, h, r))]))
        for r in (2, 1, 3, 0):
            steps.append((("down", s, h, r, 0), [], 0.1, []))
        key = ("rs", s, h)
        steps.append(
            (
                ("pair", s, h),
                [key + ("pr",)],
                0.25,
                [
                    ("x+", half, key + ("l0",), ("l0", s, h)),
                    ("x-", half, key + ("l1",), ("l1", s, h)),
                    ("x+", half, key + ("ra",), ("ra1", s, h)),
                    ("x-", half, key + ("rb",), ("rb0", s, h)),
                ],
            )
        )
        steps.append((("relay0", s, h), [key + ("l0",)], 0.1, [("x+", half, key + ("ra",), ("ra0", s, h))]))
        steps.append((("relay1", s, h), [key + ("l1",)], 0.1, [("x-", half, key + ("rb",), ("rb1", s, h))]))
        waits = [key + ("ra",), key + ("rb",)]
        if h >= 2:
            steps.append((("give", s, h), waits, 0.15, [("q", BLOCK_BYTES, ("rs", 0, h - 2, "yx"), ("yx", s, h))]))
        else:
            steps.append((("end", s, h), waits + ([key + ("yx",)] if s == 0 else []), 0.2, [("next", s)]))
    return steps


SLOTS = [(s, h) for s in range(3) for h in range(2)] + [(0, 2), (0, 3)]


@functools.lru_cache(None)
def plan():
    count = {("w", name, part): last_ones(part)[0] for name in NAMES for part in parts_of(name)}
    expected = {}
    for s, h in SLOTS:
            expected[("ag", s, h)] = 5
            expected[("rs", s, h, "yx")] = 1
            expected[("rs", s, h, "pr")] = 4
            expected[("rs", s, h, "l0")] = expected[("rs", s, h, "l1")] = 1
            expected[("rs", s, h, "ra")] = expected[("rs", s, h, "rb")] = 2
    ops, now, serial = [], 0.0, 0
    free = {link: 0.0 for link in RATE}
    ready = {link: [] for link in RATE}
    arrivals, waited = [], set()

    def offer(link, priority, size, landing, op):
        nonlocal serial
        serial += 1
        heapq.heappush(ready[link], (priority, serial, size, landing, op))

    def offer_weight(index, name, part, dy, dz):
        for link, a, b in children(part, dy, dz):
            offer(
                link,
                (index, -depth(part, a, b)),
                rows_of(name, part) * ITEMS[name][0] * 2,
                ("w", index, name, part, a, b),
                ("send", name, part, dy, dz, link, a, b),
            )

    def offer_block(s, h, at):
        for link, size, landing in gather_steps()[at]:
            offer(link, (h, s), size, ("ag", s, h, landing), ("pass", s, h, at, link))

    def pump():
        nonlocal serial
        for link, queue in ready.items():
            while queue and free[link] - now < AHEAD:
                _, _, size, landing, op = heapq.heappop(queue)
                free[link] = max(free[link], now) + size / RATE[link]
                serial += 1
                heapq.heappush(arrivals, (free[link] + DELAY.get(link, 2.3), serial, landing))
                ops.append(op)

    for name in NAMES:
        for part in parts_of(name):
            offer_weight(TURN[name], name, part, 0, 0)
    for h in range(2):
        offer("q", (0, h), BLOCK_BYTES, ("ag", 0, h + 2, "own"), ("swap", h))
        offer_block(0, h, "own")
    chains = {h: chain(h) for h in (2, 3, 0, 1)}
    times = {}
    while any(chains.values()) or arrivals or any(ready.values()):
        while arrivals and arrivals[0][0] <= now:
            _, _, landing = heapq.heappop(arrivals)
            if landing[0] == "w":
                _, index, name, part, dy, dz = landing
                if children(part, dy, dz):
                    ops.append(("got", name, part, dy, dz))
                    offer_weight(index, name, part, dy, dz)
                else:
                    count[("w", name, part)] -= 1
            elif landing[0] == "ag" and landing[3] != "end":
                ops.append(("block",) + landing[1:])
                offer_block(*landing[1:])
            else:
                key = landing[:3] if landing[0] == "ag" else landing
                expected[key] -= 1
            times[landing[:3]] = now
        pump()
        ran = False
        for h, todo in chains.items():
            if not todo:
                continue
            step, needs, duration, sends = todo[0]
            done = True
            for need in needs:
                if need[0] == "w":
                    done &= all(count[("w", need[1], part)] == 0 for part in parts_of(need[1]))
                else:
                    done &= expected[need] == 0
            if not done:
                continue
            for need in needs:
                if need not in waited:
                    waited.add(need)
                    ops.append(("all",) + need)
            ops.append(("do",) + step)
            times[step] = now
            now += duration
            todo.pop(0)
            for send in sends:
                if send[0] == "next":
                    if send[1] < 2:
                        offer_block(send[1] + 1, h, "own")
                else:
                    offer(send[0], (-1, 0), send[1], send[2], ("rsend",) + send[3])
            ran = True
            break
        if ran:
            continue
        later = [arrivals[0][0]] if arrivals else []
        later += [free[link] - AHEAD + 0.01 for link, queue in ready.items() if queue]
        if not later:
            break
        now = max(min(later), now + 0.01)
    return ops, times, now


def semaphores():
    index = {}
    for name in NAMES:
        for part in parts_of(name):
            index[("all", name, part)] = len(index)
            index[("sent", name, part)] = len(index)
    for op in plan()[0]:
        if op[0] == "got":
            index[op[1:]] = len(index)
        elif op[0] in ("block", "pass", "rsend", "swap"):
            index[op] = len(index)
    for s, h in SLOTS:
        index[("ag", s, h)] = len(index)
        for what in ("pr", "l0", "l1", "ra", "rb", "yx"):
            index[("rs", s, h, what)] = len(index)
    return index


def rms_scale(values, mean_square, gain):
    return values * lax.rsqrt(mean_square + 1e-06) * gain


def contract(left, right):
    return lax.dot_general(left, right, (((1,), (1,)), ((), ())), preferred_element_type=F32)


def kernel(sems_of, *refs):
    gate_one, up_one, down_one, proj_u, proj_v, proj_out, gate_two, up_two, down_two = refs[:9]
    resid, small_in, out = refs[9], refs[10:15], refs[15]
    g = dict(zip(NAMES, refs[16:22]))
    passing = dict(zip(SPLIT, refs[22:24]))
    (xg, normed, hidden, ps, pr, po, sb, rl, ra, rb, tt, yx, yo) = refs[24:37]
    raw, small, local_sem, sems = refs[37:43], refs[43:48], refs[48], refs[49]
    gains, spatial, bias, mix_gain, head_gain = small

    rep, fs, tp = lax.axis_index("rep"), lax.axis_index("fs"), lax.axis_index("tp")
    x, core = tp // 2, tp % 2
    y, z = fs % 8, rep * 4 + fs // 8
    odd = y % 2

    def device(link):
        if link[0] == "y":
            ny = (y + (1 if link[1] == "+" else 7)) % 8
            return {"rep": rep, "fs": (fs // 8) * 8 + ny, "tp": tp}
        if link[0] == "z":
            nz = (z + (1 if link[1] == "+" else 7)) % 8
            return {"rep": nz // 4, "fs": (nz % 4) * 8 + y, "tp": tp}
        if link[0] == "x":
            nx = (x + (1 if link[1] == "+" else 3)) % 4
            return {"rep": rep, "fs": fs, "tp": nx * 2 + core}
        if link == "q":
            return {"rep": rep, "fs": fs + 1 - 2 * odd, "tp": tp}
        return {"rep": rep, "fs": fs, "tp": x * 2 + 1 - core}

    devices = {link: device(link) for link in RATE}
    barrier = pltpu.get_barrier_semaphore()
    for link in GREET:
        pl.semaphore_signal(barrier, inc=1, device_id=devices[link], device_id_type=MESH)

    own = pl.multiple_of(fs * SHARD, SHARD)
    rows = pl.ds(own, SHARD)
    pairs = []
    for which, side in ((g, odd), (passing, 1 - odd)):
        main = pl.ds(pl.multiple_of(side * 256, 256), 256)
        pairs += [
            (gate_one.at[:, main], which["a1"].at[rows, pl.ds(0, 256)]),
            (up_one.at[:, main], which["a1"].at[rows, pl.ds(384, 256)]),
            (down_one.at[:, main], which["d1"].at[rows, pl.ds(0, 256)]),
        ]
    pairs += [
        (up_two.at[:, pl.ds(0, 640)], g["b2"].at[rows]),
        (gate_two.at[:, pl.ds(0, 640)], g["a2"].at[rows, pl.ds(0, 640)]),
        (down_two.at[:, pl.ds(0, 640)], g["d2"].at[rows]),
        (proj_out, g["m"].at[rows, pl.ds(256, 128)]),
        (proj_u, g["m"].at[rows, pl.ds(0, 128)]),
        (proj_v, g["m"].at[rows, pl.ds(128, 128)]),
        (resid, xg.at[0, tp]),
    ]
    first_copies = len(pairs)
    pairs += list(zip((gate_one, up_one, gate_two, up_two, down_one, down_two), raw))
    pairs += list(zip(small_in, small))
    copies = [pltpu.make_async_copy(src, dst, local_sem.at[k]) for k, (src, dst) in enumerate(pairs)]
    for copy in copies[first_copies:] + copies[:first_copies]:
        copy.start()
    for copy in copies[first_copies:]:
        copy.wait()
    empty = jnp.zeros((SHARD, 64), BF16)
    for name, column, k in (("a1", 256, 0), ("a1", 640, 1), ("d1", 256, 4)):
        low = raw[k][:, 512:640]
        high = jnp.concatenate([raw[k][:, 640:704], empty], axis=1)
        g[name][rows, column : column + 128] = jnp.where(odd == 0, low, high)
        passing[name][rows, column : column + 128] = jnp.where(odd == 0, high, low)
    g["a2"][rows, 640:768] = jnp.concatenate([raw[3][:, 640:704], raw[2][:, 640:704]], axis=1)
    g["m"][rows, 384:512] = jnp.concatenate([empty, raw[5][:, 640:704]], axis=1)
    pl.semaphore_wait(barrier, len(GREET))
    for copy in copies[:first_copies]:
        copy.wait()

    def piece(name, part, dy, dz, at=None):
        f = ((z + 8 - dz) % 4) * 8 + (y + 8 - dy) % 8
        start = f * SHARD + (0 if y_first(part) else ITEMS[name][1])
        array = g[name] if needed(part, dy if at is None else at) else passing[name]
        return array.at[pl.ds(pl.multiple_of(start, 16), rows_of(name, part))]

    def remote(src, dst, send, recv, link):
        return pltpu.make_async_remote_copy(
            src_ref=src,
            dst_ref=dst,
            send_sem=sems.at[sems_of[send]],
            recv_sem=sems.at[sems_of[recv]],
            device_id=devices[link],
            device_id_type=MESH,
        )

    def wait_for(ref, key):
        pltpu.make_async_copy(ref, ref, sems.at[sems_of[key]]).wait()

    def block_at(s, h, at):
        shift = {"own": 0, "m1": 3, "p1": 1, "h0": 2, "h1": 2}[at]
        start, size = (h % 2) * ROWS, ROWS
        if at[0] == "h":
            start, size = start + (0 if at == "h0" else HALF), HALF
        return xg.at[3 if h >= 2 else s, ((x + shift) % 4) * 2 + core, pl.ds(start, size)]

    def slot(s, h):
        return SLOTS.index((s, h))

    def down(s, h, r, other):
        t = ((x + r) % 4) * 2 + (1 - core if other else core)
        at = pl.ds(pl.multiple_of(t * 256, 256), 256)
        if s == 1:
            total = contract(hidden[h, :, :128], g["m"][at, 256:384])
        elif s == 0:
            total = contract(hidden[h, :, :384], g["d1"][at, :])
        else:
            total = contract(hidden[h, :, :640], g["d2"][at, :])
            total = total + contract(hidden[h, :, 640:768], g["m"][at, 384:512])
        if other:
            ps[slot(s, h), r] = total.astype(BF16)
        else:
            po[h, r] = total

    def gate_up(s, h, j):
        if s == 0:
            gate = jnp.dot(normed[h], g["a1"][:, 0:384], preferred_element_type=F32)
            up = jnp.dot(normed[h], g["a1"][:, 384:768], preferred_element_type=F32)
            hidden[h, :, :384] = (jax.nn.silu(gate) * up).astype(BF16)
            return
        a, b = g["a2"], g["b2"]
        first = jnp.dot(normed[h], a[:, 256 * j : 256 * (j + 1)], preferred_element_type=F32)
        if j < 2:
            second = jnp.dot(normed[h], b[:, 256 * j : 256 * (j + 1)], preferred_element_type=F32)
            hidden[h, :, 256 * j : 256 * (j + 1)] = (jax.nn.silu(first) * second).astype(BF16)
            return
        second = jnp.dot(normed[h], b[:, 512:640], preferred_element_type=F32)
        hidden[h, :, 512:640] = (jax.nn.silu(first[:, :128]) * second).astype(BF16)
        rest = first[:, 128:]
        value = jax.nn.silu(rest) * pltpu.roll(rest, 64, 1)
        lane = lax.broadcasted_iota(jnp.int32, (ROWS, 128), 1)
        hidden[h, :, 640:768] = jnp.where(lane >= 64, value, 0.0).astype(BF16)

    def norm(s, h):
        rows = slice((h % 2) * ROWS, (h % 2 + 1) * ROWS)
        stage, s = s, 3 if h >= 2 else s
        total = jnp.zeros((ROWS, 1), F32)
        for t in range(8):
            values = xg[s, t, rows].astype(F32)
            total = total + jnp.sum(values * values, axis=-1, keepdims=True)
        for t in range(8):
            cols = slice(256 * t, 256 * (t + 1))
            scaled = rms_scale(xg[s, t, rows].astype(F32), total / 2048.0, gains[stage : stage + 1, cols])
            normed[h, :, cols] = scaled.astype(BF16)

    def mix(h):
        both = jnp.dot(normed[h], g["m"][:, 0:256], preferred_element_type=F32)
        u, v = jax.nn.gelu(both[:, :128]), jax.nn.gelu(both[:, 128:])
        centre = jnp.mean(v, axis=-1, keepdims=True)
        spread = jnp.mean(jnp.square(v - centre), axis=-1, keepdims=True)
        vn = ((v - centre) * lax.rsqrt(spread + 1e-05) * mix_gain[...]).astype(BF16)
        to, source = lax.broadcasted_iota(jnp.int32, (128, 128), 0), lax.broadcasted_iota(jnp.int32, (128, 128), 1)
        masked = jnp.where(to // 64 >= source // 64, spatial[0].astype(F32), 0.0).astype(BF16)
        offset = jnp.sum(jnp.where(to == source, bias[...], 0.0), axis=-1, keepdims=True)
        product = u * (jnp.dot(masked, vn, preferred_element_type=F32) + offset)
        square = jnp.mean(product * product, axis=-1, keepdims=True)
        hidden[h, :, :128] = rms_scale(product, square, head_gain[...]).astype(BF16)

    lower, upper = pl.ds(0, HALF), pl.ds(HALF, HALF)
    for op in plan()[0]:
        kind = op[0]
        if kind == "send":
            _, name, part, dy, dz, link, a, b = op
            landing = (name, part, a, b) if children(part, a, b) else ("all", name, part)
            remote(piece(name, part, dy, dz), piece(name, part, dy, dz, a), ("sent", name, part), landing, link).start()
        elif kind == "swap":
            h = op[1]
            src, dst = xg.at[0, tp, pl.ds(h * ROWS, ROWS)], xg.at[3, tp, pl.ds(h * ROWS, ROWS)]
            remote(src, dst, op, ("block", 0, h + 2, "own"), "q").start()
        elif kind == "got":
            _, name, part, dy, dz = op
            wait_for(piece(name, part, dy, dz), op[1:])
        elif kind == "pass":
            _, s, h, at, link = op
            ref = block_at(s, h, at)
            if link == "d":
                landing = ("ag", s, h)
            else:
                arrived = {"own": {"x+": "m1", "x-": "p1"}, "m1": {"x+": "h0"}, "p1": {"x-": "h1"}}[at][link]
                landing = ("block", s, h, arrived)
                if at == "m1":
                    ref = ref.at[lower]
                elif at == "p1":
                    ref = ref.at[upper]
            remote(ref, ref, op, landing, link).start()
        elif kind == "block":
            wait_for(block_at(*op[1:]), op)
        elif kind == "rsend":
            what, s, h = op[1:4]
            key, k = ("rs", s, h), slot(s, h)
            if what == "pr":
                remote(ps.at[k, op[4]], pr.at[k, op[4]], op, key + ("pr",), "d").start()
            elif what == "l0":
                remote(sb.at[k, 1, lower], rl.at[k, 0], op, key + ("l0",), "x+").start()
            elif what == "l1":
                remote(sb.at[k, 1, upper], rl.at[k, 1], op, key + ("l1",), "x-").start()
            elif what == "ra1":
                remote(sb.at[k, 0, upper], ra.at[k, upper], op, key + ("ra",), "x+").start()
            elif what == "rb0":
                remote(sb.at[k, 2, lower], rb.at[k, lower], op, key + ("rb",), "x-").start()
            elif what == "ra0":
                remote(tt.at[k, 0], ra.at[k, lower], op, key + ("ra",), "x+").start()
            elif what == "rb1":
                remote(tt.at[k, 1], rb.at[k, upper], op, key + ("rb",), "x-").start()
            elif what == "yx":
                remote(yo.at[h - 2], yx.at[h - 2], op, ("rs", 0, h - 2, "yx"), "q").start()
        elif kind == "all":
            if op[1] == "w":
                name = op[2]
                for part in parts_of(name):
                    many = last_ones(part)[0] * rows_of(name, part)
                    wait_for(g[name].at[pl.ds(0, many)], ("all", name, part))
            elif op[1] == "ag":
                wait_for(xg.at[op[2], pl.ds(0, 4), pl.ds(0, ROWS)], op[1:])
            else:
                _, _, s, h, what = op
                k = slot(s, h)
                at = {"pr": pr.at[k], "l0": rl.at[k, 0], "l1": rl.at[k, 1], "ra": ra.at[k], "rb": rb.at[k], "yx": yx.at[h % 2]}
                wait_for(at[what], op[1:])
        else:
            what, s, h = op[1:4]
            k = slot(s, h)
            if what == "norm":
                norm(s, h)
            elif what == "gu":
                gate_up(s, h, op[4])
            elif what == "mix":
                mix(h)
            elif what == "down":
                down(s, h, op[4], op[5])
            elif what == "pair":
                po[h, 0] = po[h, 0] + pr[k, 0].astype(F32)
                for r in (2, 1, 3):
                    sb[k, r - 1] = (po[h, r] + pr[k, r].astype(F32)).astype(BF16)
            elif what == "relay0":
                tt[k, 0] = (sb[k, 0, :HALF].astype(F32) + rl[k, 0].astype(F32)).astype(BF16)
            elif what == "relay1":
                tt[k, 1] = (sb[k, 2, HALF:].astype(F32) + rl[k, 1].astype(F32)).astype(BF16)
            else:
                total = po[h, 0] + ra[k].astype(F32) + rb[k].astype(F32)
                if what == "give":
                    yo[h - 2] = total.astype(BF16)
                    continue
                if s == 0:
                    total = total + yx[h].astype(F32)
                at = slice(h * ROWS, (h + 1) * ROWS)
                value = (xg[s, tp, at].astype(F32) + (1.0 if s == 1 else 0.5) * total).astype(BF16)
                if s < 2:
                    xg[s + 1, tp, at] = value
                else:
                    out[at, :] = value

    for name in NAMES:
        for part in parts_of(name):
            wait_for(g[name].at[pl.ds(0, last_ones(part)[1] * rows_of(name, part))], ("sent", name, part))
    for op in plan()[0]:
        if op[0] == "pass":
            ref = block_at(op[1], op[2], op[3])
            if op[3] in ("m1", "p1") and op[4] != "d":
                ref = ref.at[lower]
            wait_for(ref, op)
        elif op[0] == "rsend":
            wait_for(ps.at[0, 0] if op[1] in ("pr", "yx") else rl.at[0, 0], op)
        elif op[0] == "swap":
            wait_for(ps.at[0, 0], op)


def body(resid, norm_gains, gate_one, up_one, down_one, proj_u, proj_v, spatial, spatial_bias, mix_gain, head_gain, proj_out, gate_two, up_two, down_two):
    weights = (gate_one, up_one, down_one.T, proj_u, proj_v, proj_out.T, gate_two, up_two, down_two.T)
    small = (norm_gains, spatial, spatial_bias, mix_gain.reshape(1, 128), head_gain.reshape(1, 128))
    raw = (gate_one, up_one, gate_two, up_two, down_one.T, down_two.T)
    sems_of = semaphores()
    rows, width = resid.shape
    return pl.pallas_call(
        functools.partial(kernel, sems_of),
        out_shape=jax.ShapeDtypeStruct((rows, width), BF16),
        in_specs=[pl.BlockSpec(memory_space=pltpu.HBM)] * 15,
        out_specs=pl.BlockSpec(memory_space=pltpu.VMEM),
        scratch_shapes=[pltpu.VMEM((2048, ITEMS[name][0]), BF16) for name in NAMES]
        + [pltpu.VMEM((2048, ITEMS[name][0]), BF16) for name in SPLIT]
        + [
            pltpu.VMEM((4, 8, 256, 256), BF16),
            pltpu.VMEM((STREAMS, ROWS, 2048), BF16),
            pltpu.VMEM((STREAMS, ROWS, 768), BF16),
            pltpu.VMEM((8, 4, ROWS, 256), BF16),
            pltpu.VMEM((8, 4, ROWS, 256), BF16),
            pltpu.VMEM((STREAMS, 4, ROWS, 256), F32),
            pltpu.VMEM((8, 3, ROWS, 256), BF16),
            pltpu.VMEM((8, 2, HALF, 256), BF16),
            pltpu.VMEM((8, ROWS, 256), BF16),
            pltpu.VMEM((8, ROWS, 256), BF16),
            pltpu.VMEM((8, 2, HALF, 256), BF16),
            pltpu.VMEM((2, ROWS, 256), BF16),
            pltpu.VMEM((2, ROWS, 256), BF16),
        ]
        + [pltpu.VMEM(a.shape, a.dtype) for a in raw + small]
        + [pltpu.SemaphoreType.DMA((24,)), pltpu.SemaphoreType.DMA((len(sems_of),))],
        compiler_params=pltpu.CompilerParams(collective_id=0, has_side_effects=True, vmem_limit_bytes=60 * 2**20),
        name="layer",
    )(*weights, resid, *small)


def solution(mesh):
    in_specs = (
        P(("rep", "fs"), "tp"),
        P(),
        P("fs", "tp"),
        P("fs", "tp"),
        P("tp", "fs"),
        P("fs", "tp"),
        P("fs", "tp"),
        P("tp", None, None),
        P("tp", None),
        P("tp"),
        P("tp"),
        P("tp", "fs"),
        P("fs", "tp"),
        P("fs", "tp"),
        P("tp", "fs"),
    )
    return jax.shard_map(body, mesh=mesh, in_specs=in_specs, out_specs=P(("rep", "fs"), "tp"), check_vma=False)
```

time: 140 us -> 132 us (0.943)
  Pallas kernels: 134 us -> 130 us
  local copies, waits for them, and re-layouts: 5.54 us -> 1.57 us
    pallas_call x1, Pallas kernels: 134 us -> 130 us  [body(): pl.pallas_call(functools.partial(kernel, sems_of), out_shape=jax.ShapeDty...]
    unnamed x6 -> x1, local copies, waits for them, and re-layouts: 5.54 us -> 1.57 us
where the time goes in v3:
time: 132 us; the launch traced here: 131 us
  Pallas kernels  130 us (98%)
  local copies, waits for them, and re-layouts  1.57 us (1%)
    pallas_call x1, Pallas kernels, body(): pl.pallas_call(functools.partial(kernel, sems_of), out_shape=jax.ShapeDty...  130 us

profile of v3, /device:TPU:1, one launch (start us, length us, event | category | flops | bytes accessed | tf_op | source)
XLA Modules:
  0.0 131.2 jit_solution(11709721085020764440)
XLA Ops:
  0.0 129.6 %layer.1 = bf16[256,256]{1,0:T(8,128)(2,1)} custom-call(bf16[64,704]{1,0:T(8,128)(2,1)} %refs_0_.1, bf16[64,704]{1,0:T(8,128)(2,1)} %refs_1_.1, bf16[64,704]{1,0:T(8,128)(2,1)} %bitcast.5, bf16[64,128]{1,0:T(8,128)(2,1)} %refs_3_.1, bf16[64,128]{1,0:T(8,128)(2,1)} %refs_4_.1, bf16[64,128]{1,0:T(8,128)(2,1)} %bitcast.7, bf16[64,704]{1,0:T(8,128)(2,1)} %refs_6_.1, ...), custom_call_target="tpu_custom_call" | custom-call | tf_op jit(solution)/shard_map/layer/pallas_call | solution.py:575
  129.7 1.6 %copy.17 = bf16[256,256]{1,0:T(8,128)(2,1)} copy(bf16[256,256]{1,0:T(8,128)(2,1)} %layer.1) | data formatting | bytes 262144

commit v4 on v3

--- a/solution.py
+++ b/solution.py
@@ -12,20 +12,19 @@
 BF16, F32 = jnp.bfloat16, jnp.float32
 SHARD = 64
 ITEMS = {
-    "a1": (768, 48),
-    "d1": (384, 48),
+    "f1": (1152, 48),
     "m": (512, 48),
-    "a2": (768, 32),
-    "b2": (640, 48),
-    "d2": (640, 32),
+    "f2a": (1024, 32),
+    "f2b": (1024, 48),
 }
 NAMES = tuple(ITEMS)
-SPLIT = ("a1", "d1")
-TURN = {"a1": 0, "d1": 0, "m": 1, "a2": 2, "b2": 2, "d2": 2}
+SPLIT = ("f1",)
+TURN = {"f1": 0, "m": 1, "f2a": 2, "f2b": 2}
 RATE = {"y+": 46600.0, "y-": 46600.0, "z+": 46600.0, "z-": 46600.0, "x+": 46600.0, "x-": 46600.0, "d": 250000.0, "q": 30000.0}
 DELAY = {"d": 1.5}
 GREET = ("y+", "y-", "z+", "z-", "x+", "x-", "d")
 AHEAD = 1.5
+LEAST = 0.5
 ROWS = 128
 HALF = 64
 BLOCK_BYTES = ROWS * 256 * 2
@@ -126,11 +125,11 @@
         if s == 1:
             steps.append((("mix", s, h), [("w", "m")], 0.7, []))
         elif s == 0:
-            steps.append((("gu", s, h, 0), [("w", "a1")], 0.5, []))
+            steps.append((("gu", s, h, 0), [("w", "f1")], 0.5, []))
         else:
             for j in range(3):
-                steps.append((("gu", s, h, j), [("w", "a2"), ("w", "b2")], 0.3, []))
-        needs = [[("w", "d1")], [("w", "m")], [("w", "m"), ("w", "d2")]][s]
+                steps.append((("gu", s, h, j), [("w", "f2a"), ("w", "f2b")], 0.3, []))
+        needs = [[("w", "f1")], [("w", "m")], [("w", "m"), ("w", "f2b")]][s]
         for r in (2, 1, 3, 0):
             steps.append((("down", s, h, r, 1), needs, 0.1, [("d", BLOCK_BYTES, ("rs", s, h, "pr"), ("pr", s, h, r))]))
         for r in (2, 1, 3, 0):
@@ -201,7 +200,10 @@
         for link, queue in ready.items():
             while queue and free[link] - now < AHEAD:
                 _, _, size, landing, op = heapq.heappop(queue)
-                free[link] = max(free[link], now) + size / RATE[link]
+                free[link] = max(free[link], now) + max(size / RATE[link], LEAST)
+                if link == "q":
+                    for shared in ("y+", "y-"):
+                        free[shared] = max(free[shared], now) + 0.5 * size / RATE[shared]
                 serial += 1
                 heapq.heappush(arrivals, (free[link] + DELAY.get(link, 2.3), serial, landing))
                 ops.append(op)
@@ -251,7 +253,7 @@
                     ops.append(("all",) + need)
             ops.append(("do",) + step)
             times[step] = now
-            now += duration
+            now += 0.6 * duration
             todo.pop(0)
             for send in sends:
                 if send[0] == "next":
@@ -300,10 +302,10 @@
 def kernel(sems_of, *refs):
     gate_one, up_one, down_one, proj_u, proj_v, proj_out, gate_two, up_two, down_two = refs[:9]
     resid, small_in, out = refs[9], refs[10:15], refs[15]
-    g = dict(zip(NAMES, refs[16:22]))
-    passing = dict(zip(SPLIT, refs[22:24]))
-    (xg, normed, hidden, ps, pr, po, sb, rl, ra, rb, tt, yx, yo) = refs[24:37]
-    raw, small, local_sem, sems = refs[37:43], refs[43:48], refs[48], refs[49]
+    g = dict(zip(NAMES, refs[16:20]))
+    passing = {"f1": refs[20]}
+    (xg, normed, hidden, ps, pr, po, sb, rl, ra, rb, tt, yx, yo) = refs[21:34]
+    raw, small, local_sem, sems = refs[34:40], refs[40:45], refs[45], refs[46]
     gains, spatial, bias, mix_gain, head_gain = small
 
     rep, fs, tp = lax.axis_index("rep"), lax.axis_index("fs"), lax.axis_index("tp")
@@ -332,42 +334,39 @@
 
     own = pl.multiple_of(fs * SHARD, SHARD)
     rows = pl.ds(own, SHARD)
-    pairs = []
-    for which, side in ((g, odd), (passing, 1 - odd)):
+    early = [(resid, xg.at[0, tp])] + list(zip((gate_one, up_one, down_one), raw[:3]))
+    for array, side in ((g["f1"], odd), (passing["f1"], 1 - odd)):
         main = pl.ds(pl.multiple_of(side * 256, 256), 256)
-        pairs += [
-            (gate_one.at[:, main], which["a1"].at[rows, pl.ds(0, 256)]),
-            (up_one.at[:, main], which["a1"].at[rows, pl.ds(384, 256)]),
-            (down_one.at[:, main], which["d1"].at[rows, pl.ds(0, 256)]),
-        ]
-    pairs += [
-        (up_two.at[:, pl.ds(0, 640)], g["b2"].at[rows]),
-        (gate_two.at[:, pl.ds(0, 640)], g["a2"].at[rows, pl.ds(0, 640)]),
-        (down_two.at[:, pl.ds(0, 640)], g["d2"].at[rows]),
-        (proj_out, g["m"].at[rows, pl.ds(256, 128)]),
+        early += [(w.at[:, main], array.at[rows, pl.ds(384 * k, 256)]) for k, w in enumerate((gate_one, up_one, down_one))]
+    late = list(zip((gate_two, up_two, down_two), raw[3:])) + [
         (proj_u, g["m"].at[rows, pl.ds(0, 128)]),
         (proj_v, g["m"].at[rows, pl.ds(128, 128)]),
-        (resid, xg.at[0, tp]),
+        (proj_out, g["m"].at[rows, pl.ds(256, 128)]),
+        (gate_two.at[:, pl.ds(0, 640)], g["f2a"].at[rows, pl.ds(0, 640)]),
+        (down_two.at[:, pl.ds(0, 256)], g["f2a"].at[rows, pl.ds(768, 256)]),
+        (up_two.at[:, pl.ds(0, 640)], g["f2b"].at[rows, pl.ds(0, 640)]),
+        (down_two.at[:, pl.ds(256, 384)], g["f2b"].at[rows, pl.ds(640, 384)]),
     ]
-    first_copies = len(pairs)
-    pairs += list(zip((gate_one, up_one, gate_two, up_two, down_one, down_two), raw))
-    pairs += list(zip(small_in, small))
-    copies = [pltpu.make_async_copy(src, dst, local_sem.at[k]) for k, (src, dst) in enumerate(pairs)]
-    for copy in copies[first_copies:] + copies[:first_copies]:
+    late += list(zip(small_in, small))
+    copies = [pltpu.make_async_copy(src, dst, local_sem.at[k]) for k, (src, dst) in enumerate(early + late)]
+    for copy in copies:
         copy.start()
-    for copy in copies[first_copies:]:
+    empty = jnp.zeros((SHARD, 64), BF16)
+    for copy in copies[: len(early)]:
         copy.wait()
-    empty = jnp.zeros((SHARD, 64), BF16)
-    for name, column, k in (("a1", 256, 0), ("a1", 640, 1), ("d1", 256, 4)):
+    for k in range(3):
         low = raw[k][:, 512:640]
         high = jnp.concatenate([raw[k][:, 640:704], empty], axis=1)
-        g[name][rows, column : column + 128] = jnp.where(odd == 0, low, high)
-        passing[name][rows, column : column + 128] = jnp.where(odd == 0, high, low)
-    g["a2"][rows, 640:768] = jnp.concatenate([raw[3][:, 640:704], raw[2][:, 640:704]], axis=1)
-    g["m"][rows, 384:512] = jnp.concatenate([empty, raw[5][:, 640:704]], axis=1)
+        column = 384 * k + 256
+        g["f1"][rows, column : column + 128] = jnp.where(odd == 0, low, high)
+        passing["f1"][rows, column : column + 128] = jnp.where(odd == 0, high, low)
     pl.semaphore_wait(barrier, len(GREET))
-    for copy in copies[:first_copies]:
-        copy.wait()
+
+    def prepare_rest():
+        for copy in copies[len(early) :]:
+            copy.wait()
+        g["f2a"][rows, 640:768] = jnp.concatenate([raw[4][:, 640:704], raw[3][:, 640:704]], axis=1)
+        g["m"][rows, 384:512] = jnp.concatenate([empty, raw[5][:, 640:704]], axis=1)
 
     def piece(name, part, dy, dz, at=None):
         f = ((z + 8 - dz) % 4) * 8 + (y + 8 - dy) % 8
@@ -404,9 +403,10 @@
         if s == 1:
             total = contract(hidden[h, :, :128], g["m"][at, 256:384])
         elif s == 0:
-            total = contract(hidden[h, :, :384], g["d1"][at, :])
+            total = contract(hidden[h, :, :384], g["f1"][at, 768:1152])
         else:
-            total = contract(hidden[h, :, :640], g["d2"][at, :])
+            total = contract(hidden[h, :, :256], g["f2a"][at, 768:1024])
+            total = total + contract(hidden[h, :, 256:640], g["f2b"][at, 640:1024])
             total = total + contract(hidden[h, :, 640:768], g["m"][at, 384:512])
         if other:
             ps[slot(s, h), r] = total.astype(BF16)
@@ -415,11 +415,11 @@
 
     def gate_up(s, h, j):
         if s == 0:
-            gate = jnp.dot(normed[h], g["a1"][:, 0:384], preferred_element_type=F32)
-            up = jnp.dot(normed[h], g["a1"][:, 384:768], preferred_element_type=F32)
+            gate = jnp.dot(normed[h], g["f1"][:, 0:384], preferred_element_type=F32)
+            up = jnp.dot(normed[h], g["f1"][:, 384:768], preferred_element_type=F32)
             hidden[h, :, :384] = (jax.nn.silu(gate) * up).astype(BF16)
             return
-        a, b = g["a2"], g["b2"]
+        a, b = g["f2a"], g["f2b"]
         first = jnp.dot(normed[h], a[:, 256 * j : 256 * (j + 1)], preferred_element_type=F32)
         if j < 2:
             second = jnp.dot(normed[h], b[:, 256 * j : 256 * (j + 1)], preferred_element_type=F32)
@@ -458,8 +458,12 @@
         hidden[h, :, :128] = rms_scale(product, square, head_gain[...]).astype(BF16)
 
     lower, upper = pl.ds(0, HALF), pl.ds(HALF, HALF)
+    prepared = False
     for op in plan()[0]:
         kind = op[0]
+        if not prepared and (kind == "got" or (kind == "send" and op[1] != "f1") or kind in ("all", "do")):
+            prepared = True
+            prepare_rest()
         if kind == "send":
             _, name, part, dy, dz, link, a, b = op
             landing = (name, part, a, b) if children(part, a, b) else ("all", name, part)
@@ -569,7 +573,7 @@
 def body(resid, norm_gains, gate_one, up_one, down_one, proj_u, proj_v, spatial, spatial_bias, mix_gain, head_gain, proj_out, gate_two, up_two, down_two):
     weights = (gate_one, up_one, down_one.T, proj_u, proj_v, proj_out.T, gate_two, up_two, down_two.T)
     small = (norm_gains, spatial, spatial_bias, mix_gain.reshape(1, 128), head_gain.reshape(1, 128))
-    raw = (gate_one, up_one, gate_two, up_two, down_one.T, down_two.T)
+    raw = (gate_one, up_one, down_one.T, gate_two, up_two, down_two.T)
     sems_of = semaphores()
     rows, width = resid.shape
     return pl.pallas_call(
@@ -595,7 +599,7 @@
             pltpu.VMEM((2, ROWS, 256), BF16),
         ]
         + [pltpu.VMEM(a.shape, a.dtype) for a in raw + small]
-        + [pltpu.SemaphoreType.DMA((24,)), pltpu.SemaphoreType.DMA((len(sems_of),))],
+        + [pltpu.SemaphoreType.DMA((25,)), pltpu.SemaphoreType.DMA((len(sems_of),))],
         compiler_params=pltpu.CompilerParams(collective_id=0, has_side_effects=True, vmem_limit_bytes=60 * 2**20),
         name="layer",
     )(*weights, resid, *small)

time: 132 us -> 130 us (0.985)
  no operation moved by 1% of the time
where the time goes in v4:
time: 130 us
  Pallas kernels  129 us (99%)
  local copies, waits for them, and re-layouts  1.57 us (1%)
    pallas_call x1, Pallas kernels, body(): pl.pallas_call(functools.partial(kernel, sems_of), out_shape=jax.ShapeDty...  129 us

profile of v4, /device:TPU:1, one launch (start us, length us, event | category | flops | bytes accessed | tf_op | source)
XLA Modules:
  0.0 130.1 jit_solution(8110903846272213364)
XLA Ops:
  0.0 128.5 %layer.1 = bf16[256,256]{1,0:T(8,128)(2,1)} custom-call(bf16[64,704]{1,0:T(8,128)(2,1)} %refs_0_.1, bf16[64,704]{1,0:T(8,128)(2,1)} %refs_1_.1, bf16[64,704]{1,0:T(8,128)(2,1)} %bitcast.5, bf16[64,128]{1,0:T(8,128)(2,1)} %refs_3_.1, bf16[64,128]{1,0:T(8,128)(2,1)} %refs_4_.1, bf16[64,128]{1,0:T(8,128)(2,1)} %bitcast.7, bf16[64,704]{1,0:T(8,128)(2,1)} %refs_6_.1, ...), custom_call_target="tpu_custom_call" | custom-call | tf_op jit(solution)/shard_map/layer/pallas_call | solution.py:579
  128.5 1.6 %copy.17 = bf16[256,256]{1,0:T(8,128)(2,1)} copy(bf16[256,256]{1,0:T(8,128)(2,1)} %layer.1) | data formatting | bytes 262144

commit v5 on v4

--- a/solution.py
+++ b/solution.py
@@ -23,7 +23,7 @@
 RATE = {"y+": 46600.0, "y-": 46600.0, "z+": 46600.0, "z-": 46600.0, "x+": 46600.0, "x-": 46600.0, "d": 250000.0, "q": 30000.0}
 DELAY = {"d": 1.5}
 GREET = ("y+", "y-", "z+", "z-", "x+", "x-", "d")
-AHEAD = 1.5
+AHEAD = 2.0
 LEAST = 0.5
 ROWS = 128
 HALF = 64

time: 130 us -> 130 us (level)
  Pallas kernels: 129 us -> 127 us
where the time goes in v5:
time: 130 us; the launch traced here: 129 us
  Pallas kernels  127 us (98%)
  local copies, waits for them, and re-layouts  1.57 us (1%)
    pallas_call x1, Pallas kernels, body(): pl.pallas_call(functools.partial(kernel, sems_of), out_shape=jax.ShapeDty...  127 us

profile of v5, /device:TPU:1, one launch (start us, length us, event | category | flops | bytes accessed | tf_op | source)
XLA Modules:
  0.0 128.8 jit_solution(15344635970949468282)
XLA Ops:
  0.0 127.2 %layer.1 = bf16[256,256]{1,0:T(8,128)(2,1)} custom-call(bf16[64,704]{1,0:T(8,128)(2,1)} %refs_0_.1, bf16[64,704]{1,0:T(8,128)(2,1)} %refs_1_.1, bf16[64,704]{1,0:T(8,128)(2,1)} %bitcast.5, bf16[64,128]{1,0:T(8,128)(2,1)} %refs_3_.1, bf16[64,128]{1,0:T(8,128)(2,1)} %refs_4_.1, bf16[64,128]{1,0:T(8,128)(2,1)} %bitcast.7, bf16[64,704]{1,0:T(8,128)(2,1)} %refs_6_.1, ...), custom_call_target="tpu_custom_call" | custom-call | tf_op jit(solution)/shard_map/layer/pallas_call | solution.py:579
  127.2 1.6 %copy.17 = bf16[256,256]{1,0:T(8,128)(2,1)} copy(bf16[256,256]{1,0:T(8,128)(2,1)} %layer.1) | data formatting | bytes 262144
